TPU v7x, 512 devices: a whole 4x4x16 slice. The times are simulated.
512 devices in a mesh: sp: 32 (over z, core), tp: 16 (over y, x).
Axes of the slice: x: 4, y: 4, z: 16, core: 2. Of those that a mesh axis runs over, the one named last changes fastest.
Arguments:
- residual_in: bfloat16 [8192, 2048], P('sp', 'tp'), may hold values from -20 to 20
- conv_value: bfloat16 [8192, 2048], P('sp', 'tp'), may hold values from -6 to 6
- conv_gate: bfloat16 [8192, 2048], P('sp', 'tp'), may hold values from -9 to 9
- doc_ids: int32 [8192], P('sp'), may hold values from 0 to 15, never falling along the last dimension, each value on 1 to 1024 neighbouring positions
- conv_kernel: bfloat16 [31, 2048], P(None, 'tp'), may hold values from -3 to 3
- ln_gain: bfloat16 [2048], P('tp'), may hold values from 0.099609375 to 1.8984375
- out_weight: bfloat16 [2048, 2048], P(None, 'tp'), may hold values from -0.25 to 0.25
- norm_gain: bfloat16 [2048], P('tp'), may hold values from 0.099609375 to 1.8984375
- routes: int32 [8192, 2], P('sp'), may hold values from 0 to 31, all different within a row; in each aligned block of 256 rows (0 to 255, 256 to 511, ...) at most 32 rows name the same one
- route_weight: float32 [8192, 2], P('sp'), may hold values from 0.1 to 1
- gate_w: bfloat16 [32, 2048, 4096], P('sp', None, 'tp'), may hold values from -0.125 to 0.125
- up_w: bfloat16 [32, 2048, 4096], P('sp', None, 'tp'), may hold values from -0.125 to 0.125
- down_w: bfloat16 [32, 4096, 2048], P('sp', 'tp'), may hold values from -0.125 to 0.125
Outputs:
- mixed: bfloat16 [8192, 2048], P('sp', 'tp')
Inputs may be any that keep to these rules, and one draw needn't show every extreme that they name: `routes`: in each aligned block of 256 positions no expert is named by more than 32 positions, a bound that some block reaches; a position's two experts differ. `doc_ids`: never falls along the positions; each document spans 1 to 1024 positions, one exactly that many.
All inputs are finite; a program needn't handle non-finite values.
Results may differ from a plain program's by a relative error of at most 0.012.
Values may be sent and summed in bfloat16 or wider, within the bound.
No kernel may reach another device: no remote copies, remote signals or barrier semaphores. Data moves between devices by JAX's collectives and lax.ppermute only.
A program may use at most 64 MiB of HBM per device.

v0:
```python
import jax
import jax.numpy as jnp
from jax import lax
from jax.sharding import Mesh
from jax.sharding import PartitionSpec as P

TP = ("tp_0", "tp_1")


epsilon = 1e-06


def from_behind(x, axis, by):
    peers = lax.axis_size(axis)
    pairs = [(i, i + by) for i in range(peers) if 0 <= i + by < peers]
    return lax.ppermute(x, axis, pairs)


def over_axes(x, axes):
    for axis in axes:
        x = lax.psum(x, axis)
    return x


def copy_for_each(x, axis):
    copies = jnp.broadcast_to(x, (lax.axis_size(axis), *x.shape))
    return lax.all_to_all(copies, axis, split_axis=0, concat_axis=0, tiled=True)


def laid_out(pieces, dim):
    lengths = list(pieces.shape[1:])
    lengths[dim] *= pieces.shape[0]
    return jnp.moveaxis(pieces, 0, dim).reshape(lengths)


def collect(x, axis, dim):
    pieces = copy_for_each(x, axis)
    return laid_out(pieces, dim)


def in_blocks(x, dim, peers):
    before, after = (x.shape[:dim], x.shape[dim + 1 :])
    return jnp.moveaxis(x.reshape(*before, peers, -1, *after), dim, 0)


def sum_at_owner(x, axis, dim):
    peers = lax.axis_size(axis)
    pieces = lax.all_to_all(in_blocks(x, dim, peers), axis, 0, 0, tiled=True)
    return jnp.sum(pieces.astype(jnp.float32), axis=0)


def per_device(
    residual_in,
    conv_value,
    conv_gate,
    doc_ids,
    conv_kernel,
    ln_gain,
    out_weight,
    norm_gain,
    routes,
    route_weight,
    gate_w,
    up_w,
    down_w,
):
    rows_here, chan_here = conv_value.shape
    lookback = conv_kernel.shape[0] - 1
    gated = (conv_value.astype(jnp.float32) * jax.nn.sigmoid(conv_gate.astype(jnp.float32))).astype(
        jnp.bfloat16
    )
    tail_values, tail_docs = from_behind(
        (gated[rows_here - lookback :], doc_ids[rows_here - lookback :]), "sp", 1
    )
    extended = jnp.concatenate([tail_values, gated], 0)
    doc_extended = jnp.concatenate([tail_docs, doc_ids], 0)
    kernel = conv_kernel.astype(jnp.float32)
    conv_out = jnp.zeros((rows_here, chan_here), jnp.float32)
    for kernel_tap in range(lookback + 1):
        same_doc = (doc_extended[kernel_tap : kernel_tap + rows_here] == doc_ids)[:, None]
        conv_out = conv_out + jnp.where(
            same_doc,
            extended[kernel_tap : kernel_tap + rows_here].astype(jnp.float32) * kernel[kernel_tap],
            0.0,
        )
    channel_sum, channel_sq = (
        over_axes(jnp.sum(conv_out, 1), TP),
        over_axes(jnp.sum(conv_out * conv_out, 1), TP),
    )
    channels = chan_here * lax.axis_size(TP)
    chan_mean = channel_sum[:, None] / channels
    chan_square = channel_sq[:, None] / channels
    activated = jax.nn.silu(
        (conv_out - chan_mean)
        * lax.rsqrt(chan_square - chan_mean * chan_mean + epsilon)
        * ln_gain.astype(jnp.float32)
    ).astype(jnp.bfloat16)
    projected = jnp.dot(
        collect(activated, TP, 1), out_weight, preferred_element_type=jnp.float32
    ).astype(jnp.bfloat16)
    stream = (residual_in.astype(jnp.float32) + projected.astype(jnp.float32)).astype(jnp.bfloat16)
    columns = stream.shape[1]
    model_width = columns * lax.axis_size(TP)
    experts = lax.axis_size("sp")
    capacity = 4 * rows_here // experts
    flat_routes = routes.reshape(-1)
    onehot = (flat_routes[:, None] == jnp.arange(experts, dtype=jnp.int32)).astype(jnp.int32)
    slot_rank = jnp.sum((jnp.cumsum(onehot, 0) - onehot) * onehot, 1)
    token_of = jnp.arange(rows_here * 2, dtype=jnp.int32) // 2
    slot_token = (
        jnp.full((experts * capacity,), rows_here, jnp.int32)
        .at[flat_routes * capacity + slot_rank]
        .set(token_of)
    )
    stream_part = stream.astype(jnp.float32)
    row_total = over_axes(jnp.sum(stream_part * stream_part, 1), TP)
    normed = (
        stream_part
        * lax.rsqrt(row_total[:, None] / model_width + epsilon)
        * norm_gain.astype(jnp.float32)
    ).astype(jnp.bfloat16)
    outbound = jnp.take(normed, slot_token, axis=0, mode="fill", fill_value=0).reshape(
        experts, capacity, columns
    )
    received = collect(
        lax.all_to_all(outbound, "sp", split_axis=0, concat_axis=0, tiled=True), TP, 2
    )
    sources, slots, features = received.shape
    gathered = received.reshape(sources * slots, features)
    hidden = (
        jax.nn.silu(jnp.dot(gathered, gate_w[0], preferred_element_type=jnp.float32))
        * jnp.dot(gathered, up_w[0], preferred_element_type=jnp.float32)
    ).astype(jnp.bfloat16)
    partial_value = jnp.dot(hidden, down_w[0], preferred_element_type=jnp.float32)
    partial_value = (
        lax.optimization_barrier(partial_value.astype(jnp.bfloat16))
        .astype(jnp.float32)
        .reshape(sources, slots, features)
    )
    summed = sum_at_owner(partial_value.astype(jnp.bfloat16), TP, 2).astype(jnp.bfloat16)
    returned = lax.all_to_all(summed, "sp", split_axis=0, concat_axis=0, tiled=True)
    pick_index = flat_routes * capacity + slot_rank
    picked = jnp.take(returned.reshape(-1, columns), pick_index, axis=0).reshape(
        rows_here, 2, columns
    )
    routed = jnp.sum(picked.astype(jnp.float32) * route_weight[:, :, None], 1)
    return (stream.astype(jnp.float32) + routed).astype(jnp.bfloat16)


def solution(mesh):
    split = Mesh(mesh.devices.reshape(mesh.shape["sp"], 4, 4), ("sp", "tp_0", "tp_1"))
    in_specs = (
        P("sp", TP),
        P("sp", TP),
        P("sp", TP),
        P("sp"),
        P(None, TP),
        P(TP),
        P(None, TP),
        P(TP),
        P("sp", None),
        P("sp", None),
        P("sp", None, TP),
        P("sp", None, TP),
        P("sp", TP, None),
    )
    out_specs = P("sp", TP)
    return jax.shard_map(
        per_device, mesh=split, in_specs=in_specs, out_specs=out_specs, check_vma=False
    )
```

profile of v0, /device:TPU:1, one launch (start us, length us, event | category | flops | bytes accessed | tf_op | source)
XLA Modules:
  0.0 283.4 jit_solution(12368834706082618189)
XLA Ops:
  0.0 0.9 slice.285
  0.9 4.9 %collective-permute-start = (s32[30]{0:T(128)S(1)}, s32[30]{0:T(128)S(1)}, u32[]{:S(2)}, u32[]{:S(2)}) collective-permute-start(s32[30]{0:T(128)S(1)} %slice.285), channel_id=1, source_target_pairs={{0,16},{16,32},{32,48},{48,64},{64,80},{80,96},{96,112},{112,128},... | collective-permute-start | bytes 368 | tf_op jit(solution)/shard_map/ppermute | solution.py:16
  5.8 0.9 multiply_convert_fusion.2
  6.7 1.9 collective-permute-start.1
  8.7 0.7 convert_element_type.165
  9.4 0.8 copy.42
  10.2 0.1 eq.146
  10.5 0.7 broadcast_multiply_fusion
  11.2 0.7 convert_element_type.196
  11.8 0.9 copy.40
  12.8 0.7 convert_element_type.204
  13.5 1.2 reduce-window.6
  14.6 0.8 pad_add_fusion
  15.4 0.8 slice_compare_fusion.29
  16.2 0.8 slice_compare_fusion.28
  16.9 1.9 fusion.68
  18.8 8.7 %all-reduce.1 = (f32[256]{0:T(256)S(1)}, f32[256]{0:T(256)S(1)}) all-reduce(f32[256]{0:T(256)S(1)} %get-tuple-element.6, f32[256]{0:T(256)S(1)} %get-tuple-element.5), channel_id=1, replica_groups=mesh['sp'=32,'tp_0'=4,'tp_1'=4] {'tp_0'}, use_global_device_ids=true, to_apply=%region_4.5 | all-reduce | flops 512 | bytes 4096 | tf_op jit(solution)/shard_map/psum | solution.py:21
  27.6 8.6 %all-reduce = (f32[256]{0:T(256)S(1)}, f32[256]{0:T(256)S(1)}) all-reduce(f32[256]{0:T(256)S(1)} %get-tuple-element.9, f32[256]{0:T(256)S(1)} %get-tuple-element.10), channel_id=1, replica_groups=mesh['sp'=32,'tp_0'=4,'tp_1'=4] {'tp_1'}, use_global_device_ids=true, to_apply=%region_5.6 | all-reduce | flops 512 | bytes 4096 | tf_op jit(solution)/shard_map/psum | solution.py:21
  36.2 0.2 multiply_convert_fusion.1
  36.4 1.1 broadcast_in_dim.293
  37.5 3.7 %all-to-all-start = ((bf16[16,256,128]{1,2,0:T(8,128)(2,1)}), bf16[16,256,128]{1,2,0:T(8,128)(2,1)S(1)}, u32[]{:S(2)}, u32[]{:S(2)}) async-start(bf16[16,256,128]{1,2,0:T(8,128)(2,1)} %broadcast_in_dim.293), calls=%async_computation | async-start | bytes 2097152 | tf_op jit(solution)/shard_map/all_to_all | solution.py:27
  41.2 0.2 slice_reduce_fusion
  41.5 0.1 copy.47
  41.6 0.1 mul.497
  41.9 2.4 scatter_custom_fusion
  44.4 10.3 %all-to-all-done = bf16[16,256,128]{1,2,0:T(8,128)(2,1)S(1)} async-done(((bf16[16,256,128]{1,2,0:T(8,128)(2,1)}), bf16[16,256,128]{1,2,0:T(8,128)(2,1)S(1)}, u32[]{:S(2)}, u32[]{:S(2)}) %all-to-all-start) | async-done | bytes 1048608 | tf_op jit(solution)/shard_map/all_to_all | solution.py:27
  54.7 0.4 multiply_reduce_fusion.1
  55.1 7.0 %psum.46 = f32[256]{0:T(256)S(1)} all-reduce(f32[256]{0:T(256)S(1)} %get-tuple-element.75), channel_id=1, replica_groups=mesh['sp'=32,'tp_0'=4,'tp_1'=4] {'tp_0'}, use_global_device_ids=true, to_apply=%region_11.12 | all-reduce | flops 256 | bytes 2048 | tf_op jit(solution)/shard_map/psum | solution.py:21
  62.1 6.0 %psum.47 = f32[256]{0:T(256)S(1)} all-reduce(f32[256]{0:T(256)S(1)} %psum.46), channel_id=1, replica_groups=mesh['sp'=32,'tp_0'=4,'tp_1'=4] {'tp_1'}, use_global_device_ids=true, to_apply=%region_12.13 | all-reduce | flops 256 | bytes 2048 | tf_op jit(solution)/shard_map/psum | solution.py:21
  68.3 3.2 %gather_fusion = bf16[1024,128]{1,0:T(8,128)(2,1)S(1)} fusion(bf16[256,128]{1,0:T(8,128)(2,1)S(1)} %copy.48, s32[1024]{0:T(1024)S(1)} %fusion.61), kind=kCustom, calls=%fused_computation | custom fusion | bytes 528384 | tf_op jit(solution)/shard_map/jit(_take)/gather | solution.py:122
  71.5 0.2 broadcast_select_fusion
  71.7 45.7 %all_to_all.25 = bf16[32,32,128]{2,1,0:T(8,128)(2,1)S(1)} all-to-all(bf16[32,32,128]{2,1,0:T(8,128)(2,1)S(1)} %broadcast_select_fusion), channel_id=1, replica_groups=mesh['sp'=32,'tp_0'=4,'tp_1'=4] {'sp'}, dimensions={0} | all-to-all | bytes 524288 | tf_op jit(solution)/shard_map/all_to_all | solution.py:126
  117.4 0.8 broadcast_in_dim.300
  118.2 52.5 %all_to_all.26 = bf16[16,32,32,128]{3,2,1,0:T(8,128)(2,1)S(1)} all-to-all(bf16[16,32,32,128]{3,2,1,0:T(8,128)(2,1)S(1)} %broadcast_in_dim.300), channel_id=1, replica_groups=mesh['sp'=32,'tp_0'=4,'tp_1'=4] {'tp_0','tp_1'}, dimensions={0} | all-to-all | bytes 8388608 | tf_op jit(solution)/shard_map/all_to_all | solution.py:27
  170.7 4.9 %copy.49 = bf16[32,32,16,128]{3,2,1,0:T(8,128)(2,1)S(1)} copy(bf16[32,32,16,128]{3,1,0,2:T(8,128)(2,1)S(1)} %bitcast.121) | data formatting | bytes 8388608 | tf_op jit(solution)/shard_map/transpose | solution.py:33
  175.6 1.9 copy-done.1
  177.5 2.3 fusion.2
  179.8 8.8 %convolution_convert_fusion = bf16[1024,2048]{1,0:T(8,128)(2,1)} fusion(bf16[128,8,16,128]{3,2,1,0:T(8,128)(2,1)} %bitcast.126, bf16[1,256,2048]{2,1,0:T(8,128)(2,1)S(1)} %copy-done, bf16[1,2048,256]{2,1,0:T(8,128)(2,1)S(1)} %copy-done.6, f32[1024,256]{1,0:T(8,128)} %fusion.2), kind=kOutput, calls=%fused_computation.8 | convolution fusion | flops 2151153664 | bytes 11534336 | tf_op jit(solution)/shard_map/dot_general | solution.py:134
  188.6 3.6 %copy.56 = bf16[128,8,16,128]{3,2,1,0:T(8,128)(2,1)S(1)} copy(bf16[128,8,16,128]{3,1,2,0:T(8,128)(2,1)} %bitcast.127) | data formatting | bytes 8388608
  192.2 1.3 copy.73
  193.5 53.1 %all_to_all.27 = bf16[16,32,32,128]{3,2,1,0:T(8,128)(2,1)} all-to-all(bf16[16,32,32,128]{3,2,1,0:T(8,128)(2,1)S(1)} %bitcast.123), channel_id=1, replica_groups=mesh['sp'=32,'tp_0'=4,'tp_1'=4] {'tp_0','tp_1'}, dimensions={0} | all-to-all | bytes 8388608 | tf_op jit(solution)/shard_map/all_to_all | solution.py:48
  246.7 3.5 %reduce_sum.67 = bf16[32,32,128]{2,1,0:T(8,128)(2,1)} reduce(bf16[16,32,32,128]{3,2,1,0:T(8,128)(2,1)} %all_to_all.27, bf16[]{:T(256)} %constant.71.clone.1), dimensions={0}, to_apply=%region_13.14 | reduce | flops 1966080 | bytes 4456450 | tf_op jit(solution)/shard_map/reduce_sum | solution.py:49
  250.2 7.2 %all-to-all-start.4 = ((bf16[32,32,128]{2,1,0:T(8,128)(2,1)}), bf16[32,32,128]{2,1,0:T(8,128)(2,1)S(1)}, u32[]{:S(2)}, u32[]{:S(2)}) async-start(bf16[32,32,128]{2,1,0:T(8,128)(2,1)} %reduce_sum.67), calls=%async_computation.4 | async-start | bytes 524288 | tf_op jit(solution)/shard_map/all_to_all | solution.py:141
  257.7 0.2 copy.46
  258.0 21.7 %all-to-all-done.4 = bf16[32,32,128]{2,1,0:T(8,128)(2,1)S(1)} async-done(((bf16[32,32,128]{2,1,0:T(8,128)(2,1)}), bf16[32,32,128]{2,1,0:T(8,128)(2,1)S(1)}, u32[]{:S(2)}, u32[]{:S(2)}) %all-to-all-start.4) | async-done | bytes 262176 | tf_op jit(solution)/shard_map/all_to_all | solution.py:141
  279.7 1.3 gather_fusion.1
  281.0 1.5 multiply_reduce_fusion
  282.6 0.7 copy.53
  (40 shorter events, 1.3 us)
Async XLA Ops:
  0.0 179.8 %copy-start = (bf16[1,256,2048]{2,1,0:T(8,128)(2,1)S(1)}, bf16[1,256,2048]{2,1,0:T(8,128)(2,1)}, u32[]{:S(2)}) copy-start(bf16[1,256,2048]{2,1,0:T(8,128)(2,1)} %param.25) | copy-start | bytes 3145732
  0.0 54.7 %copy-start.2 = (bf16[2048,128]{1,0:T(8,128)(2,1)S(1)}, bf16[2048,128]{1,0:T(8,128)(2,1)}, u32[]{:S(2)}) copy-start(bf16[2048,128]{1,0:T(8,128)(2,1)} %param.19) | copy-start | bytes 1572868
  0.9 13.8 %collective-permute-start = (s32[30]{0:T(128)S(1)}, s32[30]{0:T(128)S(1)}, u32[]{:S(2)}, u32[]{:S(2)}) collective-permute-start(s32[30]{0:T(128)S(1)} %slice.285), channel_id=1, source_target_pairs={{0,16},{16,32},{32,48},{48,64},{64,80},{80,96},{96,112},{112,128},... | collective-permute-start | bytes 368 | tf_op jit(solution)/shard_map/ppermute | solution.py:16
  6.7 10.2 %collective-permute-start.1 = (bf16[30,128]{1,0:T(8,128)(2,1)S(1)}, bf16[30,128]{1,0:T(8,128)(2,1)S(1)}, u32[]{:S(2)}, u32[]{:S(2)}) collective-permute-start(bf16[30,128]{1,0:T(8,128)(2,1)S(1)} %slice.384), channel_id=1, source_target_pairs={{0,16},{16,32},{32,48},{48,64},{64,80},{80,96},{96,112},{112,128},... | collective-permute-start | bytes 23048 | tf_op jit(solution)/shard_map/ppermute | solution.py:16
  37.5 17.2 %all-to-all-start = ((bf16[16,256,128]{1,2,0:T(8,128)(2,1)}), bf16[16,256,128]{1,2,0:T(8,128)(2,1)S(1)}, u32[]{:S(2)}, u32[]{:S(2)}) async-start(bf16[16,256,128]{1,2,0:T(8,128)(2,1)} %broadcast_in_dim.293), calls=%async_computation | async-start | bytes 2097152 | tf_op jit(solution)/shard_map/all_to_all | solution.py:27
  170.7 6.8 %copy-start.5 = (bf16[1,2048,256]{2,1,0:T(8,128)(2,1)S(1)}, bf16[1,2048,256]{2,1,0:T(8,128)(2,1)}, u32[]{:S(2)}) copy-start(bf16[1,2048,256]{2,1,0:T(8,128)(2,1)} %param.23) | copy-start | bytes 3145732
  175.6 1.9 copy-start.1
  177.5 2.3 copy-start.6
  246.6 11.0 %copy-start.3 = (s32[256,2]{0,1:T(2,128)S(1)}, s32[256,2]{0,1:T(2,128)}, u32[]{:S(2)}) copy-start(s32[256,2]{0,1:T(2,128)} %param.21) | copy-start | bytes 6148
  246.7 11.2 %copy-start.4 = (f32[256,2]{0,1:T(2,128)S(1)}, f32[256,2]{0,1:T(2,128)}, u32[]{:S(2)}) copy-start(f32[256,2]{0,1:T(2,128)} %param.22) | copy-start | bytes 6148
  250.2 29.5 %all-to-all-start.4 = ((bf16[32,32,128]{2,1,0:T(8,128)(2,1)}), bf16[32,32,128]{2,1,0:T(8,128)(2,1)S(1)}, u32[]{:S(2)}, u32[]{:S(2)}) async-start(bf16[32,32,128]{2,1,0:T(8,128)(2,1)} %reduce_sum.67), calls=%async_computation.4 | async-start | bytes 524288 | tf_op jit(solution)/shard_map/all_to_all | solution.py:141
where the time goes:
time: 284 us; the launch traced here: 283 us
  blocking collectives  182 us (64%)
  waiting for transfers between devices  32 us (11%)
  local copies, waits for them, and re-layouts  25.6 us (9%)
  starting transfers between devices  17.7 us (6%)
  other arithmetic  14.6 us (5%)
  matrix products  11.5 us (4%)
    all_to_all x1, blocking collectives, sum_at_owner(): pieces = lax.all_to_all(in_blocks(x, dim, peers), axis, 0, 0, tiled=True)  53.1 us
    all_to_all x1, blocking collectives, copy_for_each(): return lax.all_to_all(copies, axis, split_axis=0, concat_axis=0, tiled=True)  52.5 us
    all_to_all x1, blocking collectives, per_device(): lax.all_to_all(outbound, 'sp', split_axis=0, concat_axis=0, tiled=True)  45.7 us
    psum x4, blocking collectives, over_axes(): x = lax.psum(x, axis)  30.3 us
    all_to_all x1, waiting for transfers between devices, per_device(): lax.all_to_all(summed, 'sp', split_axis=0, concat_axis=0, tiled=True)  21.7 us
    all_to_all x1, waiting for transfers between devices, copy_for_each(): return lax.all_to_all(copies, axis, split_axis=0, concat_axis=0, tiled=True)  10.3 us
    dot_general x1, matrix products, per_device(): jnp.dot(hidden, down_w[0], preferred_element_type=jnp.float32)  8.8 us
    unnamed x18, local copies, waits for them, and re-layouts  7.4 us
  transfers between devices with their start and end apart: 4, of which 2 were waited for; matrix products, arithmetic and copies ran while one was open for 5% of the time, Pallas kernels for 0%

commit v1 on v0

v1 whole, which is shorter than its diff:
```python
import jax
import jax.numpy as jnp
from jax import lax
from jax.experimental import pallas as pl
from jax.experimental.pallas import tpu as pltpu
from jax.sharding import Mesh
from jax.sharding import PartitionSpec as P

TP = ("tp_0", "tp_1")
epsilon = 1e-06
F32 = jnp.float32
BF16 = jnp.bfloat16
HALO = 32
EXTRA = 16


def in_vmem():
    return pl.BlockSpec(memory_space=pltpu.VMEM)


def call(kernel, outs, scratch=(), flops=0, name=None):
    return pl.pallas_call(
        kernel,
        out_shape=outs,
        out_specs=jax.tree.map(lambda _: in_vmem(), outs),
        scratch_shapes=list(scratch),
        name=name,
        cost_estimate=pl.CostEstimate(flops=flops, bytes_accessed=1 << 20, transcendentals=0),
        compiler_params=pltpu.CompilerParams(vmem_limit_bytes=48 * 2**20),
    )


def shape(dims, dtype=BF16):
    return jax.ShapeDtypeStruct(dims, dtype)


def down_lanes(row):
    return jnp.concatenate(
        [
            jnp.transpose(jnp.broadcast_to(row[:, i : i + 128], (128, 128)))
            for i in range(0, row.shape[1], 128)
        ],
        0,
    )


def gate_of(value, gate):
    return (value.astype(F32) * jax.nn.sigmoid(gate.astype(F32))).astype(BF16)


def tail_kernel(value, gate, docs, out):
    rows = value.shape[0]
    out[:HALO] = gate_of(value[rows - HALO :], gate[rows - HALO :])
    last = docs[docs.shape[0] - 1 :].astype(F32)
    out[HALO:] = down_lanes(last)[128 - HALO :].astype(BF16)


def conv_kernel(value, gate, docs, halo, taps, ln_gain, norm_gain, out, gext, dext):
    rows, chans = value.shape
    ntaps = taps.shape[0]
    gext[:HALO] = halo[:HALO].astype(F32)
    gext[HALO:] = gate_of(value[...], gate[...]).astype(F32)
    dext[:HALO] = halo[HALO:].astype(F32)
    for i in range(rows // 128):
        dext[HALO + 128 * i : HALO + 128 * (i + 1)] = down_lanes(docs[i : i + 1].astype(F32))
    kernel = taps[...].astype(F32)
    first = HALO - ntaps + 1
    step = 64
    means = []
    for r in range(0, rows, step):
        doc = dext[HALO + r : HALO + r + step]
        acc = jnp.zeros((step, chans), F32)
        for j in range(ntaps):
            at = first + j + r
            acc = acc + jnp.where(
                dext[at : at + step] == doc, gext[at : at + step] * kernel[j : j + 1], 0.0
            )
        mean = jnp.mean(acc, 1, keepdims=True)
        out[r : r + step] = (acc - mean).astype(BF16)
        means.append(jnp.broadcast_to(mean, (step, 128)))
    lines = []
    for i in range(rows // 128):
        lines.append(jnp.transpose(jnp.concatenate(means[2 * i : 2 * i + 2], 0))[:1])
    mean = jnp.concatenate(lines, 0)
    high = mean.astype(BF16).astype(F32)
    low = mean - high
    tail = jnp.concatenate(
        [high, low, ln_gain[...].astype(F32), norm_gain[...].astype(F32)], 0
    )
    tail = jnp.concatenate([tail, jnp.zeros((EXTRA - tail.shape[0], 128), F32)], 0)
    out[rows:] = tail.astype(BF16)


def routing_kernel(routes, weights, rank_out, pick_out, weight_out):
    rows = routes.shape[1]
    experts = rank_out.shape[0]
    capacity = 4 * rows // experts
    expert = lax.broadcasted_iota(jnp.int32, (experts, rows), 0)
    first = routes[:1] == expert
    second = routes[1:] == expert
    named = jnp.logical_or(first, second)
    before = lax.broadcasted_iota(jnp.int32, (rows, rows), 0) < lax.broadcasted_iota(
        jnp.int32, (rows, rows), 1
    )
    rank = jnp.dot(
        named.astype(F32).astype(BF16),
        before.astype(F32).astype(BF16),
        preferred_element_type=F32,
    )
    rank_out[...] = jnp.where(named, rank, -1.0)
    slot = rank + (expert * capacity).astype(F32)
    for k, chosen in enumerate((first, second)):
        pick = jnp.sum(jnp.where(chosen, slot, 0.0), 0, keepdims=True)
        pick_out[k] = down_lanes(pick)
        weight_out[k] = down_lanes(weights[k : k + 1])


def stream_kernel(parts, out_weight, residual, rank, stream_out, sent, means, full, act, place):
    peers, extended, chans = parts.shape
    rows = extended - EXTRA
    width = peers * chans
    for d in range(peers):
        tail = parts[d, rows:].astype(F32)
        for i in range(rows // 128):
            means[d : d + 1, 128 * i : 128 * (i + 1)] = tail[i : i + 1]
            means[peers + d : peers + d + 1, 128 * i : 128 * (i + 1)] = tail[
                rows // 128 + i : rows // 128 + i + 1
            ]
    owner = lax.broadcasted_iota(jnp.int32, (2 * peers, width), 0)
    block = lax.broadcasted_iota(jnp.int32, (2 * peers, width), 1) // chans
    spread = jnp.logical_or(owner == block, owner == block + peers).astype(F32).astype(BF16)
    full[...] = lax.dot_general(
        means[...].astype(BF16),
        spread,
        (((0,), (0,)), ((), ())),
        preferred_element_type=F32,
    )
    nextra = 2 * (rows // 128)
    step = 64
    for r in range(0, rows, step):
        total = jnp.zeros((step, chans), F32)
        square = jnp.zeros((step, chans), F32)
        for d in range(peers):
            x = full[r : r + step, d * chans : (d + 1) * chans] + parts[d, r : r + step].astype(F32)
            full[r : r + step, d * chans : (d + 1) * chans] = x
            total = total + x
            square = square + x * x
        mean = jnp.sum(total, 1, keepdims=True) / width
        var = jnp.sum(square, 1, keepdims=True) / width - mean * mean
        scale = lax.rsqrt(var + epsilon)
        for d in range(peers):
            gain = parts[d, rows:].astype(F32)[nextra : nextra + 1]
            x = full[r : r + step, d * chans : (d + 1) * chans]
            x = (x - mean) * scale * gain
            act[r : r + step, d * chans : (d + 1) * chans] = (x / (1.0 + jnp.exp(-x))).astype(BF16)
    projected = jnp.dot(act[...], out_weight[...], preferred_element_type=F32).astype(BF16)
    stream = (residual[...].astype(F32) + projected.astype(F32)).astype(BF16)
    stream_out[...] = stream
    experts, capacity, _ = sent.shape
    slot = lax.broadcasted_iota(jnp.int32, (capacity, rows), 0).astype(F32)
    for e in range(experts):
        place[e * capacity : (e + 1) * capacity] = (
            (rank[e : e + 1] == slot).astype(F32).astype(BF16)
        )
    moved = jnp.dot(place[...], stream, preferred_element_type=F32).astype(BF16)
    sent[...] = moved.reshape(sent.shape)


def expert_kernel(parts, gains, gate_a, up_a, down_a, gate_b, up_b, down_b, out, normed):
    peers, rows, chans = parts.shape
    width = peers * chans
    step = 64
    for r in range(0, rows, step):
        square = jnp.zeros((step, chans), F32)
        for d in range(peers):
            x = parts[d, r : r + step].astype(F32)
            square = square + x * x
        scale = lax.rsqrt(jnp.sum(square, 1, keepdims=True) / width + epsilon)
        for d in range(peers):
            x = parts[d, r : r + step].astype(F32) * scale * gains[d : d + 1].astype(F32)
            normed[r : r + step, d * chans : (d + 1) * chans] = x.astype(BF16)
    step = 256
    for r in range(0, rows, step):
        x = normed[r : r + step]
        hidden = []
        for gate_w, up_w in ((gate_a, up_a), (gate_b, up_b)):
            gate = jnp.dot(x, gate_w[...], preferred_element_type=F32)
            up = jnp.dot(x, up_w[...], preferred_element_type=F32)
            hidden.append((gate / (1.0 + jnp.exp(-gate)) * up).astype(BF16))
        for c in range(0, width, 512):
            y = jnp.dot(hidden[0], down_a[:, c : c + 512], preferred_element_type=F32)
            y = y + jnp.dot(hidden[1], down_b[:, c : c + 512], preferred_element_type=F32)
            y = y.astype(BF16)
            for i in range(512 // chans):
                out[c // chans + i, r : r + step] = y[:, i * chans : (i + 1) * chans]


def mix_kernel(returned, pick, weight, stream, out):
    rows = stream.shape[0]
    slots = returned.shape[0]
    lane = lax.broadcasted_iota(jnp.int32, (rows, 128), 1).astype(F32)
    routed = jnp.zeros(stream.shape, F32)
    back = returned[...]
    for k in range(2):
        choose = jnp.concatenate(
            [
                (pick[k] == lane + float(s)).astype(F32).astype(BF16)
                for s in range(0, slots, 128)
            ],
            1,
        )
        picked = jnp.dot(choose, back, preferred_element_type=F32)
        routed = routed + picked * weight[k]
    out[...] = (stream[...].astype(F32) + routed).astype(BF16)


def to_each(x, axis):
    copies = jnp.broadcast_to(x, (lax.axis_size(axis), *x.shape))
    return lax.all_to_all(copies, axis, split_axis=0, concat_axis=0, tiled=True)


def swap_pair(x):
    peers = lax.axis_size("tp_1")
    return lax.ppermute(x, "tp_1", [(i, i ^ 1) for i in range(peers)])


def per_device(
    residual_in,
    conv_value,
    conv_gate,
    doc_ids,
    conv_kernel_w,
    ln_gain,
    out_weight,
    norm_gain,
    routes,
    route_weight,
    gate_w,
    up_w,
    down_w,
):
    rows, chans = conv_value.shape
    experts = lax.axis_size("sp")
    peers = lax.axis_size(TP)
    capacity = 4 * rows // experts
    slots = experts * capacity
    width = peers * chans
    docs = doc_ids.reshape(rows // 128, 128)
    gate_a, up_a, down_a = gate_w[0], up_w[0], down_w[0]

    tail = call(tail_kernel, shape((2 * HALO, chans)), name="tail")(conv_value, conv_gate, docs)
    n = lax.axis_size("sp")
    halo = lax.ppermute(tail, "sp", [(i, i + 1) for i in range(n - 1)])
    gate_b, up_b, down_b = swap_pair(gate_a), swap_pair(up_a), swap_pair(down_a)
    packed = call(
        conv_kernel,
        shape((rows + EXTRA, chans)),
        [pltpu.VMEM((rows + HALO, chans), F32), pltpu.VMEM((rows + HALO, chans), F32)],
        name="conv",
    )(
        conv_value,
        conv_gate,
        docs,
        halo,
        conv_kernel_w,
        ln_gain.reshape(1, chans),
        norm_gain.reshape(1, chans),
    )
    rank, pick, weight = call(
        routing_kernel,
        (shape((experts, rows), F32), shape((2, rows, 128), F32), shape((2, rows, 128), F32)),
        name="routing",
    )(routes.T, route_weight.T)
    parts = to_each(packed, TP)
    stream, sent = call(
        stream_kernel,
        (shape((rows, chans)), shape((experts, capacity, chans))),
        [
            pltpu.VMEM((2 * peers, rows), F32),
            pltpu.VMEM((rows, width), F32),
            pltpu.VMEM((rows, width), BF16),
            pltpu.VMEM((slots, rows), BF16),
        ],
        name="stream",
    )(parts, out_weight, residual_in, rank)
    gains = parts[:, rows + 2 * (rows // 128) + 1, :]
    received = lax.all_to_all(sent, "sp", split_axis=0, concat_axis=0, tiled=True)
    half = slots // 2
    outbound = jnp.broadcast_to(
        received.reshape(1, 2, half, chans), (peers // 2, 2, half, chans)
    ).reshape(peers, half, chans)
    gathered = lax.all_to_all(outbound, TP, split_axis=0, concat_axis=0, tiled=True)
    partial = call(
        expert_kernel,
        shape((peers, half, chans)),
        [pltpu.VMEM((half, width), BF16)],
        name="expert",
    )(gathered, gains, gate_a, up_a, down_a, gate_b, up_b, down_b)
    pieces = lax.all_to_all(partial, TP, split_axis=0, concat_axis=0, tiled=True)
    summed = jnp.sum(pieces.reshape(peers // 2, 2, half, chans).astype(F32), 0).astype(BF16)
    returned = lax.all_to_all(
        summed.reshape(experts, capacity, chans), "sp", split_axis=0, concat_axis=0, tiled=True
    )
    return call(mix_kernel, shape((rows, chans)), name="mix")(
        returned.reshape(slots, chans), pick, weight, stream
    )


def solution(mesh):
    split = Mesh(mesh.devices.reshape(mesh.shape["sp"], 4, 4), ("sp", "tp_0", "tp_1"))
    in_specs = (
        P("sp", TP),
        P("sp", TP),
        P("sp", TP),
        P("sp"),
        P(None, TP),
        P(TP),
        P(None, TP),
        P(TP),
        P("sp", None),
        P("sp", None),
        P("sp", None, TP),
        P("sp", None, TP),
        P("sp", TP, None),
    )
    out_specs = P("sp", TP)
    return jax.shard_map(
        per_device, mesh=split, in_specs=in_specs, out_specs=out_specs, check_vma=False
    )
```

time: 284 us -> 258 us (0.908)
  blocking collectives: 182 us -> 99.2 us
  waiting for transfers between devices: 32 us -> 109 us
  other arithmetic: 14.6 us -> 0.4 us
  matrix products: 11.5 us -> 0 us
  Pallas kernels: 0 us -> 11.3 us
  local copies, waits for them, and re-layouts: 25.6 us -> 16 us
  starting transfers between devices: 17.7 us -> 21.6 us
    ppermute x2 -> x4, waiting for transfers between devices: 0.01 us -> 90.3 us  [the longest x3 86.5 us: swap_pair(): return lax.ppermute(x, 'tp_1', [(i, i ^ 1) for i in range(peers)])]
    all_to_all x3, blocking collectives: 151 us -> 99.2 us  [the longest x1 37.8 us: per_device(): lax.all_to_all(sent, 'sp', split_axis=0, concat_axis=0, tiled=True)]
    psum x4 -> x0, blocking collectives: 30.3 us -> none  [over_axes(): x = lax.psum(x, axis)]
    all_to_all x2, waiting for transfers between devices: 32 us -> 18.5 us  [the longest x1 18.5 us: to_each(): return lax.all_to_all(copies, axis, split_axis=0, concat_axis=0, tiled=True)]
    dot_general x3 -> x0, matrix products: 11.5 us -> none  [the longest x1 8.8 us: per_device(): jnp.dot(hidden, down_w[0], preferred_element_type=jnp.float32)]
    pallas_call x0 -> x6, Pallas kernels: none -> 11.3 us  [the longest x1 6.92 us: per_device(): call(expert_kernel, shape((peers, half, chans)), [pltpu.VMEM((half, width...]
    reduce_sum x4 -> x1, other arithmetic: 6.95 us -> 0.4 us  [per_device(): jnp.sum(pieces.reshape(peers // 2, 2, half, chans).astype(F32), 0)]
    ppermute x2 -> x4, starting transfers between devices: 6.83 us -> 13.3 us  [the longest x3 8.37 us: swap_pair(): return lax.ppermute(x, 'tp_1', [(i, i ^ 1) for i in range(peers)])]
  transfers between devices with their start and end apart: 4 -> 6, of which waited for: 2 -> 5; matrix products, arithmetic and copies ran while one was open for 5% -> 0% of each run, Pallas kernels for 0% -> 0%
where the time goes in v1:
time: 258 us; the launch traced here: 257 us
  waiting for transfers between devices  109 us (42%)
  blocking collectives  99.2 us (38%)
  starting transfers between devices  21.6 us (8%)
  local copies, waits for them, and re-layouts  16 us (6%)
  Pallas kernels  11.3 us (4%)
    ppermute x3, waiting for transfers between devices, swap_pair(): return lax.ppermute(x, 'tp_1', [(i, i ^ 1) for i in range(peers)])  86.5 us
    all_to_all x1, blocking collectives, per_device(): lax.all_to_all(sent, 'sp', split_axis=0, concat_axis=0, tiled=True)  37.8 us
    all_to_all x1, blocking collectives, per_device(): lax.all_to_all(partial, TP, split_axis=0, concat_axis=0, tiled=True)  32.4 us
    all_to_all x1, blocking collectives, per_device(): lax.all_to_all(summed.reshape(experts, capacity, chans), 'sp', split_axis...  29 us
    all_to_all x1, waiting for transfers between devices, to_each(): return lax.all_to_all(copies, axis, split_axis=0, concat_axis=0, tiled=True)  18.5 us
    unnamed x45, local copies, waits for them, and re-layouts  13.1 us
    ppermute x3, starting transfers between devices, swap_pair(): return lax.ppermute(x, 'tp_1', [(i, i ^ 1) for i in range(peers)])  8.37 us
    pallas_call x1, Pallas kernels, per_device(): call(expert_kernel, shape((peers, half, chans)), [pltpu.VMEM((half, width...  6.92 us
  transfers between devices with their start and end apart: 6, of which 5 were waited for; matrix products, arithmetic and copies ran while one was open for 0% of the time, Pallas kernels for 0%

profile of v1, /device:TPU:1, one launch (start us, length us, event | category | flops | bytes accessed | tf_op | source)
XLA Modules:
  0.0 257.5 jit_solution(14008605546659092994)
XLA Ops:
  0.0 0.0 copy-start.7
  0.0 0.9 copy-done.10
  0.9 0.8 copy-done.12
  1.7 0.7 copy-done.16
  2.4 0.1 tail.1
  2.5 4.9 %collective-permute-start = (bf16[64,128]{1,0:T(8,128)(2,1)S(1)}, bf16[64,128]{1,0:T(8,128)(2,1)S(1)}, u32[]{:S(2)}, u32[]{:S(2)}) collective-permute-start(bf16[64,128]{1,0:T(8,128)(2,1)S(1)} %tail.1), channel_id=1, source_target_pairs={{0,16},{16,32},{32,48},{48,64},{64,80},{80,96},{96,112},{112,128},... | collective-permute-start | bytes 49160 | tf_op jit(solution)/shard_map/ppermute | solution.py:253
  7.4 3.9 %collective-permute-done.halo = bf16[64,128]{1,0:T(8,128)(2,1)S(1)} collective-permute-done((bf16[64,128]{1,0:T(8,128)(2,1)S(1)}, bf16[64,128]{1,0:T(8,128)(2,1)S(1)}, u32[]{:S(2)}, u32[]{:S(2)}) %collective-permute-start) | collective-permute-done | bytes 16416 | tf_op jit(solution)/shard_map/ppermute | solution.py:253
  11.3 0.8 copy-done.11
  12.1 0.8 copy-done.13
  13.0 0.7 copy-done.15
  13.7 0.7 copy-done.17
  14.4 0.7 copy-done.20
  15.0 0.7 copy-done.21
  15.7 0.9 conv.1
  16.5 1.2 broadcast_in_dim.10
  17.7 3.7 %all-to-all-start = ((bf16[16,272,128]{2,1,0:T(8,128)(2,1)}), bf16[16,272,128]{2,1,0:T(8,128)(2,1)S(1)}, u32[]{:S(2)}, u32[]{:S(2)}) async-start(bf16[16,272,128]{2,1,0:T(8,128)(2,1)} %broadcast_in_dim.10), calls=%async_computation | async-start | bytes 2228224 | tf_op jit(solution)/shard_map/all_to_all | solution.py:219
  21.5 0.0 copy-done.18
  21.5 0.0 copy-done.19
  21.5 0.3 routing.1
  21.8 0.0 copy-start.8
  21.8 0.7 copy-done.8
  22.5 18.5 %all-to-all-done.parts = bf16[16,272,128]{2,1,0:T(8,128)(2,1)S(1)} async-done(((bf16[16,272,128]{2,1,0:T(8,128)(2,1)}), bf16[16,272,128]{2,1,0:T(8,128)(2,1)S(1)}, u32[]{:S(2)}, u32[]{:S(2)}) %all-to-all-start) | async-done | bytes 1114144 | tf_op jit(solution)/shard_map/all_to_all | solution.py:219
  41.0 0.0 copy-done.7
  41.0 0.0 copy-done.14
  41.0 2.0 stream.1
  43.0 37.8 %all_to_all.25 = bf16[32,32,128]{2,1,0:T(8,128)(2,1)S(1)} all-to-all(bf16[32,32,128]{2,1,0:T(8,128)(2,1)S(1)} %get-tuple-element.11), channel_id=1, replica_groups=mesh['sp'=32,'tp_0'=4,'tp_1'=4] {'sp'}, dimensions={0} | all-to-all | bytes 524288 | tf_op jit(solution)/shard_map/all_to_all | solution.py:287
  80.9 1.7 broadcast_in_dim.12
  82.6 4.6 %all-to-all-start.2 = ((bf16[16,512,128]{2,1,0:T(8,128)(2,1)}), bf16[16,512,128]{2,1,0:T(8,128)(2,1)}, u32[]{:S(2)}, u32[]{:S(2)}) async-start(bf16[16,512,128]{2,1,0:T(8,128)(2,1)} %bitcast.31), calls=%async_computation.2 | async-start | bytes 4194304 | tf_op jit(solution)/shard_map/all_to_all | solution.py:292
  87.1 0.0 copy-done
  87.2 3.1 %collective-permute-start.1 = (bf16[2048,256]{1,0:T(8,128)(2,1)S(1)}, bf16[2048,256]{1,0:T(8,128)(2,1)S(1)}, u32[]{:S(2)}, u32[]{:S(2)}) collective-permute-start(bf16[2048,256]{1,0:T(8,128)(2,1)S(1)} %bitcast.16), channel_id=1, source_target_pairs={{0,1},{1,0},{2,3},{3,2},{4,5},{5,4},{6,7},{7,6},{8,9},{9,8},{10,11... | collective-permute-start | bytes 3145736 | tf_op jit(solution)/shard_map/ppermute | solution.py:224
  90.2 0.0 copy-done.1
  90.3 2.2 collective-permute-start.2
  92.5 3.1 %collective-permute-start.3 = (bf16[256,2048]{1,0:T(8,128)(2,1)}, bf16[256,2048]{1,0:T(8,128)(2,1)}, u32[]{:S(2)}, u32[]{:S(2)}) collective-permute-start(bf16[256,2048]{1,0:T(8,128)(2,1)} %bitcast.20), channel_id=1, source_target_pairs={{0,1},{1,0},{2,3},{3,2},{4,5},{5,4},{6,7},{7,6},{8,9},{9,8},{10,11... | collective-permute-start | bytes 3145736 | tf_op jit(solution)/shard_map/ppermute | solution.py:224
  95.6 43.4 %collective-permute-done.1.gate_b = bf16[2048,256]{1,0:T(8,128)(2,1)S(1)} collective-permute-done((bf16[2048,256]{1,0:T(8,128)(2,1)S(1)}, bf16[2048,256]{1,0:T(8,128)(2,1)S(1)}, u32[]{:S(2)}, u32[]{:S(2)}) %collective-permute-start.1) | collective-permute-done | bytes 1048608 | tf_op jit(solution)/shard_map/ppermute | solution.py:224
  139.0 1.0 copy-done.3
  140.0 21.5 %collective-permute-done.2.up_b = bf16[2048,256]{1,0:T(8,128)(2,1)S(1)} collective-permute-done((bf16[2048,256]{1,0:T(8,128)(2,1)S(1)}, bf16[2048,256]{1,0:T(8,128)(2,1)S(1)}, u32[]{:S(2)}, u32[]{:S(2)}) %collective-permute-start.2) | collective-permute-done | bytes 1048608 | tf_op jit(solution)/shard_map/ppermute | solution.py:224
  161.4 1.0 copy-done.5
  162.4 21.6 %collective-permute-done.3.down_b = bf16[256,2048]{1,0:T(8,128)(2,1)} collective-permute-done((bf16[256,2048]{1,0:T(8,128)(2,1)}, bf16[256,2048]{1,0:T(8,128)(2,1)}, u32[]{:S(2)}, u32[]{:S(2)}) %collective-permute-start.3) | collective-permute-done | bytes 1048608 | tf_op jit(solution)/shard_map/ppermute | solution.py:224
  184.0 0.0 all-to-all-done.2.parts
  184.0 1.2 copy-done.2
  185.3 1.2 copy-done.4
  186.5 1.2 copy-done.6
  187.7 6.9 %expert.1 = bf16[16,512,128]{2,1,0:T(8,128)(2,1)} custom-call(bf16[16,512,128]{2,1,0:T(8,128)(2,1)} %all-to-all-done.2.parts, bf16[16,128]{1,0:T(8,128)(2,1)S(1)} %bitcast.23, bf16[2048,256]{1,0:T(8,128)(2,1)S(1)} %bitcast.17, bf16[2048,256]{1,0:T(8,128)(2,1)S(1)} %bitcast.19, bf16[256,2048]{1,0:T(8,128)(2,1)S(1)} %bitcast.21, ...), custom_call_target="tpu_custom_call" | custom-call | bytes 1048576 | tf_op jit(solution)/shard_map/expert/pallas_call | solution.py:293
  194.6 32.4 %all_to_all.26 = bf16[16,512,128]{2,1,0:T(8,128)(2,1)S(1)} all-to-all(bf16[16,512,128]{2,1,0:T(8,128)(2,1)} %expert.1), channel_id=1, replica_groups=mesh['sp'=32,'tp_0'=4,'tp_1'=4] {'tp_0','tp_1'}, dimensions={0} | all-to-all | bytes 4194304 | tf_op jit(solution)/shard_map/all_to_all | solution.py:299
  227.0 0.4 reduce_sum.12
  227.4 29.0 %all_to_all.27 = bf16[32,32,128]{2,1,0:T(8,128)(2,1)S(1)} all-to-all(bf16[32,32,128]{2,1,0:T(8,128)(2,1)S(1)} %bitcast.32), channel_id=1, replica_groups=mesh['sp'=32,'tp_0'=4,'tp_1'=4] {'sp'}, dimensions={0} | all-to-all | bytes 524288 | tf_op jit(solution)/shard_map/all_to_all | solution.py:301
  256.4 0.0 copy-done.9
  256.4 1.1 mix.1
  (22 shorter events, 0.0 us)
Async XLA Ops:
  0.0 41.0 %copy-start.7 = (bf16[2048,128]{1,0:T(8,128)(2,1)S(1)}, bf16[2048,128]{1,0:T(8,128)(2,1)}, u32[]{:S(2)}) copy-start(bf16[2048,128]{1,0:T(8,128)(2,1)} %out_weight.1) | copy-start | bytes 1572868
  0.0 0.9 copy-start.10
  0.9 0.8 copy-start.12
  1.7 0.7 copy-start.16
  2.5 8.8 %collective-permute-start = (bf16[64,128]{1,0:T(8,128)(2,1)S(1)}, bf16[64,128]{1,0:T(8,128)(2,1)S(1)}, u32[]{:S(2)}, u32[]{:S(2)}) collective-permute-start(bf16[64,128]{1,0:T(8,128)(2,1)S(1)} %tail.1), channel_id=1, source_target_pairs={{0,16},{16,32},{32,48},{48,64},{64,80},{80,96},{96,112},{112,128},... | collective-permute-start | bytes 49160 | tf_op jit(solution)/shard_map/ppermute | solution.py:253
  11.3 0.8 copy-start.11
  12.1 0.8 copy-start.13
  13.0 0.7 copy-start.15
  13.7 0.7 copy-start.17
  14.4 0.7 copy-start.20
  15.0 0.7 copy-start.21
  15.7 5.8 %copy-start.18 = (s32[256,2]{0,1:T(2,128)S(1)}, s32[256,2]{0,1:T(2,128)}, u32[]{:S(2)}) copy-start(s32[256,2]{0,1:T(2,128)} %param.21) | copy-start | bytes 6148
  15.7 5.8 %copy-start.19 = (f32[256,2]{0,1:T(2,128)S(1)}, f32[256,2]{0,1:T(2,128)}, u32[]{:S(2)}) copy-start(f32[256,2]{0,1:T(2,128)} %param.22) | copy-start | bytes 6148
  15.7 25.3 %copy-start.14 = (bf16[256,128]{1,0:T(8,128)(2,1)S(1)}, bf16[256,128]{1,0:T(8,128)(2,1)}, u32[]{:S(2)}) copy-start(bf16[256,128]{1,0:T(8,128)(2,1)} %residual.1) | copy-start | bytes 196612
  17.7 23.3 %all-to-all-start = ((bf16[16,272,128]{2,1,0:T(8,128)(2,1)}), bf16[16,272,128]{2,1,0:T(8,128)(2,1)S(1)}, u32[]{:S(2)}, u32[]{:S(2)}) async-start(bf16[16,272,128]{2,1,0:T(8,128)(2,1)} %broadcast_in_dim.10), calls=%async_computation | async-start | bytes 2228224 | tf_op jit(solution)/shard_map/all_to_all | solution.py:219
  21.8 0.7 copy-start.8
  82.6 4.6 %copy-start = (bf16[1,2048,256]{2,1,0:T(8,128)(2,1)S(1)}, bf16[1,2048,256]{2,1,0:T(8,128)(2,1)}, u32[]{:S(2)}) copy-start(bf16[1,2048,256]{2,1,0:T(8,128)(2,1)} %param.23) | copy-start | bytes 3145732
  82.6 7.7 %copy-start.1 = (bf16[1,2048,256]{2,1,0:T(8,128)(2,1)S(1)}, bf16[1,2048,256]{2,1,0:T(8,128)(2,1)}, u32[]{:S(2)}) copy-start(bf16[1,2048,256]{2,1,0:T(8,128)(2,1)} %param.24) | copy-start | bytes 3145732
  82.6 101.5 %all-to-all-start.2 = ((bf16[16,512,128]{2,1,0:T(8,128)(2,1)}), bf16[16,512,128]{2,1,0:T(8,128)(2,1)}, u32[]{:S(2)}, u32[]{:S(2)}) async-start(bf16[16,512,128]{2,1,0:T(8,128)(2,1)} %bitcast.31), calls=%async_computation.2 | async-start | bytes 4194304 | tf_op jit(solution)/shard_map/all_to_all | solution.py:292
  87.2 51.8 %collective-permute-start.1 = (bf16[2048,256]{1,0:T(8,128)(2,1)S(1)}, bf16[2048,256]{1,0:T(8,128)(2,1)S(1)}, u32[]{:S(2)}, u32[]{:S(2)}) collective-permute-start(bf16[2048,256]{1,0:T(8,128)(2,1)S(1)} %bitcast.16), channel_id=1, source_target_pairs={{0,1},{1,0},{2,3},{3,2},{4,5},{5,4},{6,7},{7,6},{8,9},{9,8},{10,11... | collective-permute-start | bytes 3145736 | tf_op jit(solution)/shard_map/ppermute | solution.py:224
  90.3 71.2 %collective-permute-start.2 = (bf16[2048,256]{1,0:T(8,128)(2,1)S(1)}, bf16[2048,256]{1,0:T(8,128)(2,1)S(1)}, u32[]{:S(2)}, u32[]{:S(2)}) collective-permute-start(bf16[2048,256]{1,0:T(8,128)(2,1)S(1)} %bitcast.18), channel_id=1, source_target_pairs={{0,1},{1,0},{2,3},{3,2},{4,5},{5,4},{6,7},{7,6},{8,9},{9,8},{10,11... | collective-permute-start | bytes 3145736 | tf_op jit(solution)/shard_map/ppermute | solution.py:224
  92.5 91.6 %collective-permute-start.3 = (bf16[256,2048]{1,0:T(8,128)(2,1)}, bf16[256,2048]{1,0:T(8,128)(2,1)}, u32[]{:S(2)}, u32[]{:S(2)}) collective-permute-start(bf16[256,2048]{1,0:T(8,128)(2,1)} %bitcast.20), channel_id=1, source_target_pairs={{0,1},{1,0},{2,3},{3,2},{4,5},{5,4},{6,7},{7,6},{8,9},{9,8},{10,11... | collective-permute-start | bytes 3145736 | tf_op jit(solution)/shard_map/ppermute | solution.py:224
  139.0 1.0 copy-start.3
  161.4 1.0 copy-start.5
  184.0 1.2 copy-start.2
  185.3 1.2 copy-start.4
  186.5 1.2 copy-start.6
  227.0 29.4 %copy-start.9 = (f32[2,256,128]{2,1,0:T(8,128)S(1)}, f32[2,256,128]{2,1,0:T(8,128)}, u32[]{:S(2)}) copy-start(f32[2,256,128]{2,1,0:T(8,128)} %copy-done.8) | copy-start | bytes 786436

commit v2 on v1

--- a/solution.py
+++ b/solution.py
@@ -6,6 +6,7 @@
 from jax.sharding import Mesh
 from jax.sharding import PartitionSpec as P
 
+
 TP = ("tp_0", "tp_1")
 epsilon = 1e-06
 F32 = jnp.float32
@@ -14,20 +15,41 @@
 EXTRA = 16
 
 
-def in_vmem():
-    return pl.BlockSpec(memory_space=pltpu.VMEM)
-
-
-def call(kernel, outs, scratch=(), flops=0, name=None):
+def vmem(dims, dtype=BF16):
+    return pltpu.VMEM(dims, dtype)
+
+
+def call(kernel, outs, ins, scratch=(), copies=0, spread=False, flops=0):
+    space = {"h": pltpu.HBM, "v": pltpu.VMEM}
+    sems = [pltpu.SemaphoreType.DMA((copies,))] if copies else []
+    out_space = pltpu.HBM if spread else pltpu.VMEM
     return pl.pallas_call(
         kernel,
         out_shape=outs,
-        out_specs=jax.tree.map(lambda _: in_vmem(), outs),
-        scratch_shapes=list(scratch),
-        name=name,
+        in_specs=[pl.BlockSpec(memory_space=space[c]) for c in ins],
+        out_specs=jax.tree.map(lambda _: pl.BlockSpec(memory_space=out_space), outs),
+        scratch_shapes=list(scratch) + sems,
         cost_estimate=pl.CostEstimate(flops=flops, bytes_accessed=1 << 20, transcendentals=0),
         compiler_params=pltpu.CompilerParams(vmem_limit_bytes=48 * 2**20),
     )
+
+
+def start(pairs, sems, first=0):
+    made = [
+        pltpu.make_async_copy(src, dst, sems.at[first + i]) for i, (src, dst) in enumerate(pairs)
+    ]
+    for copy in made:
+        copy.start()
+    return made
+
+
+def finish(made):
+    for copy in made:
+        copy.wait()
+
+
+def half_of(core, peer):
+    return jnp.where(core == 0, peer % 2, (peer // 4) % 2)
 
 
 def shape(dims, dtype=BF16):
@@ -48,14 +70,56 @@
     return (value.astype(F32) * jax.nn.sigmoid(gate.astype(F32))).astype(BF16)
 
 
-def tail_kernel(value, gate, docs, out):
-    rows = value.shape[0]
-    out[:HALO] = gate_of(value[rows - HALO :], gate[rows - HALO :])
+def tail_kernel(value_h, gate_h, docs_h, out, value, gate, docs, sems):
+    rows = value_h.shape[0]
+    finish(
+        start(
+            [
+                (value_h.at[rows - HALO :], value),
+                (gate_h.at[rows - HALO :], gate),
+                (docs_h, docs),
+            ],
+            sems,
+        )
+    )
+    out[:HALO] = gate_of(value[...], gate[...])
     last = docs[docs.shape[0] - 1 :].astype(F32)
     out[HALO:] = down_lanes(last)[128 - HALO :].astype(BF16)
 
 
-def conv_kernel(value, gate, docs, halo, taps, ln_gain, norm_gain, out, gext, dext):
+def conv_kernel(
+    halo,
+    value_h,
+    gate_h,
+    docs_h,
+    taps_h,
+    ln_gain_h,
+    norm_gain_h,
+    sent,
+    value,
+    gate,
+    docs,
+    taps,
+    ln_gain,
+    norm_gain,
+    gext,
+    dext,
+    out,
+    sems,
+):
+    finish(
+        start(
+            [
+                (value_h, value),
+                (gate_h, gate),
+                (docs_h, docs),
+                (taps_h, taps),
+                (ln_gain_h, ln_gain),
+                (norm_gain_h, norm_gain),
+            ],
+            sems,
+        )
+    )
     rows, chans = value.shape
     ntaps = taps.shape[0]
     gext[:HALO] = halo[:HALO].astype(F32)
@@ -89,6 +153,7 @@
     )
     tail = jnp.concatenate([tail, jnp.zeros((EXTRA - tail.shape[0], 128), F32)], 0)
     out[rows:] = tail.astype(BF16)
+    finish(start([(out, sent.at[i]) for i in range(sent.shape[0])], sems))
 
 
 def routing_kernel(routes, weights, rank_out, pick_out, weight_out):
@@ -166,7 +231,46 @@
     sent[...] = moved.reshape(sent.shape)
 
 
-def expert_kernel(parts, gains, gate_a, up_a, down_a, gate_b, up_b, down_b, out, normed):
+def spread_kernel(received, out, sems):
+    core = lax.axis_index("sp") % 2
+    peers, half, _ = out.shape
+    pairs = []
+    for i in range(peers):
+        first = pl.multiple_of(half_of(core, i) * half, half)
+        pairs.append((received.at[pl.ds(first, half)], out.at[i]))
+    finish(start(pairs, sems))
+
+
+def expert_kernel(
+    parts,
+    gains,
+    gate_ah,
+    up_ah,
+    down_ah,
+    gate_bh,
+    up_bh,
+    down_bh,
+    out,
+    normed,
+    gate_a,
+    up_a,
+    down_a,
+    gate_b,
+    up_b,
+    down_b,
+    sems,
+):
+    made = start(
+        [
+            (gate_ah, gate_a),
+            (up_ah, up_a),
+            (gate_bh, gate_b),
+            (up_bh, up_b),
+            (down_ah, down_a),
+            (down_bh, down_b),
+        ],
+        sems,
+    )
     peers, rows, chans = parts.shape
     width = peers * chans
     step = 64
@@ -179,6 +283,7 @@
         for d in range(peers):
             x = parts[d, r : r + step].astype(F32) * scale * gains[d : d + 1].astype(F32)
             normed[r : r + step, d * chans : (d + 1) * chans] = x.astype(BF16)
+    finish(made)
     step = 256
     for r in range(0, rows, step):
         x = normed[r : r + step]
@@ -193,6 +298,18 @@
             y = y.astype(BF16)
             for i in range(512 // chans):
                 out[c // chans + i, r : r + step] = y[:, i * chans : (i + 1) * chans]
+
+
+def sum_kernel(pieces, out):
+    core = lax.axis_index("sp") % 2
+    peers, half, _ = pieces.shape
+    for h in range(2):
+        total = jnp.zeros(pieces.shape[1:], F32)
+        for k in range(peers // 2):
+            across = (k // 2) * 4 + (k % 2) * 2 + h
+            down = ((k // 4) * 2 + h) * 4 + k % 4
+            total = total + pieces[jnp.where(core == 0, across, down)].astype(F32)
+        out[h * half : (h + 1) * half] = total.astype(BF16)
 
 
 def mix_kernel(returned, pick, weight, stream, out):
@@ -214,14 +331,18 @@
     out[...] = (stream[...].astype(F32) + routed).astype(BF16)
 
 
-def to_each(x, axis):
-    copies = jnp.broadcast_to(x, (lax.axis_size(axis), *x.shape))
-    return lax.all_to_all(copies, axis, split_axis=0, concat_axis=0, tiled=True)
+def exchange(x, axis):
+    return lax.all_to_all(x, axis, split_axis=0, concat_axis=0, tiled=True)
 
 
 def swap_pair(x):
-    peers = lax.axis_size("tp_1")
-    return lax.ppermute(x, "tp_1", [(i, i ^ 1) for i in range(peers)])
+    groups, peers = lax.axis_size("sp"), lax.axis_size(TP)
+    pairs = [
+        (s * peers + t, s * peers + (t ^ (1 if s % 2 == 0 else 4)))
+        for s in range(groups)
+        for t in range(peers)
+    ]
+    return lax.ppermute(x, ("sp", *TP), pairs)
 
 
 def per_device(
@@ -248,20 +369,40 @@
     docs = doc_ids.reshape(rows // 128, 128)
     gate_a, up_a, down_a = gate_w[0], up_w[0], down_w[0]
 
-    tail = call(tail_kernel, shape((2 * HALO, chans)), name="tail")(conv_value, conv_gate, docs)
+    tail = call(
+        tail_kernel,
+        shape((2 * HALO, chans)),
+        "hhh",
+        [vmem((HALO, chans)), vmem((HALO, chans)), vmem(docs.shape, jnp.int32)],
+        copies=3,
+    )(conv_value, conv_gate, docs)
     n = lax.axis_size("sp")
     halo = lax.ppermute(tail, "sp", [(i, i + 1) for i in range(n - 1)])
-    gate_b, up_b, down_b = swap_pair(gate_a), swap_pair(up_a), swap_pair(down_a)
+    gate_b = swap_pair(gate_a)
+    up_b = swap_pair(up_a)
+    down_b = swap_pair(down_a)
     packed = call(
         conv_kernel,
-        shape((rows + EXTRA, chans)),
-        [pltpu.VMEM((rows + HALO, chans), F32), pltpu.VMEM((rows + HALO, chans), F32)],
-        name="conv",
+        shape((peers, rows + EXTRA, chans)),
+        "vhhhhhh",
+        [
+            vmem((rows, chans)),
+            vmem((rows, chans)),
+            vmem(docs.shape, jnp.int32),
+            vmem(conv_kernel_w.shape),
+            vmem((1, chans)),
+            vmem((1, chans)),
+            vmem((rows + HALO, chans), F32),
+            vmem((rows + HALO, chans), F32),
+            vmem((rows + EXTRA, chans)),
+        ],
+        copies=peers,
+        spread=True,
     )(
+        halo,
         conv_value,
         conv_gate,
         docs,
-        halo,
         conv_kernel_w,
         ln_gain.reshape(1, chans),
         norm_gain.reshape(1, chans),
@@ -269,39 +410,39 @@
     rank, pick, weight = call(
         routing_kernel,
         (shape((experts, rows), F32), shape((2, rows, 128), F32), shape((2, rows, 128), F32)),
-        name="routing",
+        "vv",
     )(routes.T, route_weight.T)
-    parts = to_each(packed, TP)
+    parts = exchange(packed, TP)
     stream, sent = call(
         stream_kernel,
         (shape((rows, chans)), shape((experts, capacity, chans))),
+        "vvvv",
         [
-            pltpu.VMEM((2 * peers, rows), F32),
-            pltpu.VMEM((rows, width), F32),
-            pltpu.VMEM((rows, width), BF16),
-            pltpu.VMEM((slots, rows), BF16),
+            vmem((2 * peers, rows), F32),
+            vmem((rows, width), F32),
+            vmem((rows, width)),
+            vmem((slots, rows)),
         ],
-        name="stream",
     )(parts, out_weight, residual_in, rank)
     gains = parts[:, rows + 2 * (rows // 128) + 1, :]
-    received = lax.all_to_all(sent, "sp", split_axis=0, concat_axis=0, tiled=True)
+    received = exchange(sent, "sp")
     half = slots // 2
-    outbound = jnp.broadcast_to(
-        received.reshape(1, 2, half, chans), (peers // 2, 2, half, chans)
-    ).reshape(peers, half, chans)
-    gathered = lax.all_to_all(outbound, TP, split_axis=0, concat_axis=0, tiled=True)
+    outbound = call(
+        spread_kernel, shape((peers, half, chans)), "v", copies=peers, spread=True
+    )(received.reshape(slots, chans))
+    gathered = exchange(outbound, TP)
     partial = call(
         expert_kernel,
         shape((peers, half, chans)),
-        [pltpu.VMEM((half, width), BF16)],
-        name="expert",
+        "vvhhhhhh",
+        [vmem((half, width))]
+        + [vmem(gate_a.shape), vmem(up_a.shape), vmem(down_a.shape)] * 2,
+        copies=6,
     )(gathered, gains, gate_a, up_a, down_a, gate_b, up_b, down_b)
-    pieces = lax.all_to_all(partial, TP, split_axis=0, concat_axis=0, tiled=True)
-    summed = jnp.sum(pieces.reshape(peers // 2, 2, half, chans).astype(F32), 0).astype(BF16)
-    returned = lax.all_to_all(
-        summed.reshape(experts, capacity, chans), "sp", split_axis=0, concat_axis=0, tiled=True
-    )
-    return call(mix_kernel, shape((rows, chans)), name="mix")(
+    pieces = exchange(partial, TP)
+    summed = call(sum_kernel, shape((slots, chans)), "v")(pieces)
+    returned = exchange(summed.reshape(experts, capacity, chans), "sp")
+    return call(mix_kernel, shape((rows, chans)), "vvvv")(
         returned.reshape(slots, chans), pick, weight, stream
     )
 

time: 258 us -> 221 us (0.86)
  waiting for transfers between devices: 109 us -> 70.9 us
  Pallas kernels: 11.3 us -> 16.5 us
  local copies, waits for them, and re-layouts: 16 us -> 13.1 us
    ppermute x3, waiting for transfers between devices: 86.5 us -> 48.6 us  [swap_pair(): return lax.ppermute(x, ('sp', *TP), pairs)]
    pallas_call x4 -> x6, Pallas kernels: 8.97 us -> 14.1 us  [the longest x1 8.89 us: per_device(): call(expert_kernel, shape((peers, half, chans)), 'vvhhhhhh', [vmem((half,...]
    broadcast_in_dim x2 -> x0, local copies, waits for them, and re-layouts: 2.9 us -> none  [the longest x1 1.71 us: per_device(): jnp.broadcast_to(received.reshape(1, 2, half, chans), (peers // 2, 2, hal...]
where the time goes in v2:
time: 221 us
  blocking collectives  98.2 us (44%)
  waiting for transfers between devices  70.9 us (32%)
  starting transfers between devices  21.7 us (10%)
  Pallas kernels  16.5 us (7%)
  local copies, waits for them, and re-layouts  13.1 us (6%)
    all_to_all x3, blocking collectives, exchange(): return lax.all_to_all(x, axis, split_axis=0, concat_axis=0, tiled=True)  98.2 us
    ppermute x3, waiting for transfers between devices, swap_pair(): return lax.ppermute(x, ('sp', *TP), pairs)  48.6 us
    all_to_all x2, waiting for transfers between devices, exchange(): return lax.all_to_all(x, axis, split_axis=0, concat_axis=0, tiled=True)  18.5 us
    unnamed x45, local copies, waits for them, and re-layouts  13.1 us
    pallas_call x1, Pallas kernels, per_device(): call(expert_kernel, shape((peers, half, chans)), 'vvhhhhhh', [vmem((half,...  8.89 us
    ppermute x3, starting transfers between devices, swap_pair(): return lax.ppermute(x, ('sp', *TP), pairs)  8.39 us
    all_to_all x2, starting transfers between devices, exchange(): return lax.all_to_all(x, axis, split_axis=0, concat_axis=0, tiled=True)  8.34 us
    ppermute x1, starting transfers between devices, per_device(): halo = lax.ppermute(tail, 'sp', [(i, i + 1) for i in range(n - 1)])  4.92 us
  transfers between devices with their start and end apart: 6, of which 5 were waited for; matrix products, arithmetic and copies ran while one was open for 0% of the time, Pallas kernels for 0%

profile of v2, /device:TPU:1, one launch (start us, length us, event | category | flops | bytes accessed | tf_op | source)
XLA Modules:
  0.0 220.5 jit_solution(14693673119218422441)
XLA Ops:
  0.0 0.9 copy-done.10
  0.9 0.8 copy-done.12
  1.7 0.7 copy-done.16
  2.4 0.1 shard_map.127
  2.6 4.9 %collective-permute-start = (bf16[64,128]{1,0:T(8,128)(2,1)S(1)}, bf16[64,128]{1,0:T(8,128)(2,1)S(1)}, u32[]{:S(2)}, u32[]{:S(2)}) collective-permute-start(bf16[64,128]{1,0:T(8,128)(2,1)S(1)} %shard_map.127), channel_id=1, source_target_pairs={{0,16},{16,32},{32,48},{48,64},{64,80},{80,96},{96,112},{112,128},... | collective-permute-start | bytes 49160 | tf_op jit(solution)/shard_map/ppermute | solution.py:380
  7.5 3.9 %collective-permute-done.halo = bf16[64,128]{1,0:T(8,128)(2,1)S(1)} collective-permute-done((bf16[64,128]{1,0:T(8,128)(2,1)S(1)}, bf16[64,128]{1,0:T(8,128)(2,1)S(1)}, u32[]{:S(2)}, u32[]{:S(2)}) %collective-permute-start) | collective-permute-done | bytes 16416 | tf_op jit(solution)/shard_map/ppermute | solution.py:380
  11.4 0.8 copy-done.11
  12.2 0.8 copy-done.13
  13.0 0.7 copy-done.15
  13.7 0.7 copy-done.17
  14.4 0.7 copy-done.20
  15.1 0.7 copy-done.21
  15.7 2.2 %shard_map.128 = bf16[16,272,128]{2,1,0:T(8,128)(2,1)} custom-call(bf16[64,128]{1,0:T(8,128)(2,1)S(1)} %collective-permute-done.halo, bf16[256,128]{1,0:T(8,128)(2,1)S(1)} %copy-done.11, bf16[256,128]{1,0:T(8,128)(2,1)S(1)} %copy-done.13, s32[2,128]{1,0:T(2,128)S(1)} %bitcast.25, bf16[31,128]{1,0:T(8,128)(2,1)S(1)} %copy-done.15, ...), custom_call_target="tpu_custom_call" | custom-call | bytes 1048576 | tf_op jit(solution)/shard_map/pallas_call | solution.py:384
  18.0 3.8 %all-to-all-start = ((bf16[16,272,128]{2,1,0:T(8,128)(2,1)}), bf16[16,272,128]{2,1,0:T(8,128)(2,1)S(1)}, u32[]{:S(2)}, u32[]{:S(2)}) async-start(bf16[16,272,128]{2,1,0:T(8,128)(2,1)} %shard_map.128), calls=%async_computation | async-start | bytes 2228224 | tf_op jit(solution)/shard_map/all_to_all | solution.py:335
  21.8 0.0 copy-done.18
  21.8 0.0 copy-done.19
  21.8 0.3 shard_map.129
  22.1 0.0 copy-start.8
  22.1 0.7 copy-done.8
  22.8 18.5 %all-to-all-done.parts = bf16[16,272,128]{2,1,0:T(8,128)(2,1)S(1)} async-done(((bf16[16,272,128]{2,1,0:T(8,128)(2,1)}), bf16[16,272,128]{2,1,0:T(8,128)(2,1)S(1)}, u32[]{:S(2)}, u32[]{:S(2)}) %all-to-all-start) | async-done | bytes 1114144 | tf_op jit(solution)/shard_map/all_to_all | solution.py:335
  41.3 0.0 copy-done.7
  41.3 0.0 copy-done.14
  41.3 2.0 shard_map.130
  43.3 37.8 %all_to_all.25 = bf16[32,32,128]{2,1,0:T(8,128)(2,1)S(1)} all-to-all(bf16[32,32,128]{2,1,0:T(8,128)(2,1)S(1)} %get-tuple-element.11), channel_id=1, replica_groups=mesh['sp'=32,'tp_0'=4,'tp_1'=4] {'sp'}, dimensions={0} | all-to-all | bytes 524288 | tf_op jit(solution)/shard_map/all_to_all | solution.py:335
  81.1 1.5 shard_map.131
  82.6 0.0 copy-start
  82.6 0.0 copy-start.1
  82.6 4.6 %all-to-all-start.2 = ((bf16[16,512,128]{2,1,0:T(8,128)(2,1)}), bf16[16,512,128]{2,1,0:T(8,128)(2,1)}, u32[]{:S(2)}, u32[]{:S(2)}) async-start(bf16[16,512,128]{2,1,0:T(8,128)(2,1)} %shard_map.131), calls=%async_computation.2 | async-start | bytes 4194304 | tf_op jit(solution)/shard_map/all_to_all | solution.py:335
  87.2 0.0 copy-done
  87.2 3.1 %collective-permute-start.1 = (bf16[2048,256]{1,0:T(8,128)(2,1)S(1)}, bf16[2048,256]{1,0:T(8,128)(2,1)S(1)}, u32[]{:S(2)}, u32[]{:S(2)}) collective-permute-start(bf16[2048,256]{1,0:T(8,128)(2,1)S(1)} %bitcast.14), channel_id=1, source_target_pairs={{0,1},{1,0},{2,3},{3,2},{4,5},{5,4},{6,7},{7,6},{8,9},{9,8},{10,11... | collective-permute-start | bytes 3145736 | tf_op jit(solution)/shard_map/ppermute | solution.py:345
  90.3 0.0 copy-done.1
  90.3 2.2 collective-permute-start.2
  92.5 3.1 %collective-permute-start.3 = (bf16[256,2048]{1,0:T(8,128)(2,1)}, bf16[256,2048]{1,0:T(8,128)(2,1)}, u32[]{:S(2)}, u32[]{:S(2)}) collective-permute-start(bf16[256,2048]{1,0:T(8,128)(2,1)} %bitcast.18), channel_id=1, source_target_pairs={{0,1},{1,0},{2,3},{3,2},{4,5},{5,4},{6,7},{7,6},{8,9},{9,8},{10,11... | collective-permute-start | bytes 3145736 | tf_op jit(solution)/shard_map/ppermute | solution.py:345
  95.7 27.9 %collective-permute-done.1.gate_bh = bf16[2048,256]{1,0:T(8,128)(2,1)S(1)} collective-permute-done((bf16[2048,256]{1,0:T(8,128)(2,1)S(1)}, bf16[2048,256]{1,0:T(8,128)(2,1)S(1)}, u32[]{:S(2)}, u32[]{:S(2)}) %collective-permute-start.1) | collective-permute-done | bytes 1048608 | tf_op jit(solution)/shard_map/ppermute | solution.py:345
  123.6 1.0 copy-done.3
  124.6 10.2 %collective-permute-done.2.up_bh = bf16[2048,256]{1,0:T(8,128)(2,1)S(1)} collective-permute-done((bf16[2048,256]{1,0:T(8,128)(2,1)S(1)}, bf16[2048,256]{1,0:T(8,128)(2,1)S(1)}, u32[]{:S(2)}, u32[]{:S(2)}) %collective-permute-start.2) | collective-permute-done | bytes 1048608 | tf_op jit(solution)/shard_map/ppermute | solution.py:345
  134.8 1.0 copy-done.5
  135.8 10.4 %collective-permute-done.3.down_bh = bf16[256,2048]{1,0:T(8,128)(2,1)} collective-permute-done((bf16[256,2048]{1,0:T(8,128)(2,1)}, bf16[256,2048]{1,0:T(8,128)(2,1)}, u32[]{:S(2)}, u32[]{:S(2)}) %collective-permute-start.3) | collective-permute-done | bytes 1048608 | tf_op jit(solution)/shard_map/ppermute | solution.py:345
  146.2 0.0 all-to-all-done.2.parts
  146.2 1.2 copy-done.2
  147.4 1.2 copy-done.4
  148.6 1.2 copy-done.6
  149.9 8.9 %shard_map.132 = bf16[16,512,128]{2,1,0:T(8,128)(2,1)} custom-call(bf16[16,512,128]{2,1,0:T(8,128)(2,1)} %all-to-all-done.2.parts, bf16[16,128]{1,0:T(8,128)(2,1)S(1)} %bitcast.23, bf16[2048,256]{1,0:T(8,128)(2,1)S(1)} %bitcast.15, bf16[2048,256]{1,0:T(8,128)(2,1)S(1)} %bitcast.17, bf16[256,2048]{1,0:T(8,128)(2,1)S(1)} %bitcast.19, ...), custom_call_target="tpu_custom_call" | custom-call | bytes 1048576 | tf_op jit(solution)/shard_map/pallas_call | solution.py:434
  158.8 30.3 %all_to_all.26.pieces = bf16[16,512,128]{2,1,0:T(8,128)(2,1)S(1)} all-to-all(bf16[16,512,128]{2,1,0:T(8,128)(2,1)} %shard_map.132), channel_id=1, replica_groups=mesh['sp'=32,'tp_0'=4,'tp_1'=4] {'tp_0','tp_1'}, dimensions={0} | all-to-all | bytes 4194304 | tf_op jit(solution)/shard_map/all_to_all | solution.py:335
  189.1 0.3 shard_map.133
  189.4 30.0 %all_to_all.27 = bf16[32,32,128]{2,1,0:T(8,128)(2,1)S(1)} all-to-all(bf16[32,32,128]{2,1,0:T(8,128)(2,1)S(1)} %bitcast.22), channel_id=1, replica_groups=mesh['sp'=32,'tp_0'=4,'tp_1'=4] {'sp'}, dimensions={0} | all-to-all | bytes 524288 | tf_op jit(solution)/shard_map/all_to_all | solution.py:335
  219.4 0.0 copy-done.9
  219.4 1.1 shard_map.134
  (21 shorter events, 0.0 us)
Async XLA Ops:
  0.0 41.3 %copy-start.7 = (bf16[2048,128]{1,0:T(8,128)(2,1)S(1)}, bf16[2048,128]{1,0:T(8,128)(2,1)}, u32[]{:S(2)}) copy-start(bf16[2048,128]{1,0:T(8,128)(2,1)} %out_weight.1) | copy-start | bytes 1572868
  0.0 0.9 copy-start.10
  0.9 0.8 copy-start.12
  1.7 0.7 copy-start.16
  2.6 8.8 %collective-permute-start = (bf16[64,128]{1,0:T(8,128)(2,1)S(1)}, bf16[64,128]{1,0:T(8,128)(2,1)S(1)}, u32[]{:S(2)}, u32[]{:S(2)}) collective-permute-start(bf16[64,128]{1,0:T(8,128)(2,1)S(1)} %shard_map.127), channel_id=1, source_target_pairs={{0,16},{16,32},{32,48},{48,64},{64,80},{80,96},{96,112},{112,128},... | collective-permute-start | bytes 49160 | tf_op jit(solution)/shard_map/ppermute | solution.py:380
  11.4 0.8 copy-start.11
  12.2 0.8 copy-start.13
  13.0 0.7 copy-start.15
  13.7 0.7 copy-start.17
  14.4 0.7 copy-start.20
  15.1 0.7 copy-start.21
  15.7 6.0 %copy-start.18 = (s32[256,2]{0,1:T(2,128)S(1)}, s32[256,2]{0,1:T(2,128)}, u32[]{:S(2)}) copy-start(s32[256,2]{0,1:T(2,128)} %param.21) | copy-start | bytes 6148
  15.7 6.0 %copy-start.19 = (f32[256,2]{0,1:T(2,128)S(1)}, f32[256,2]{0,1:T(2,128)}, u32[]{:S(2)}) copy-start(f32[256,2]{0,1:T(2,128)} %param.22) | copy-start | bytes 6148
  15.7 25.5 %copy-start.14 = (bf16[256,128]{1,0:T(8,128)(2,1)S(1)}, bf16[256,128]{1,0:T(8,128)(2,1)}, u32[]{:S(2)}) copy-start(bf16[256,128]{1,0:T(8,128)(2,1)} %residual.1) | copy-start | bytes 196612
  18.0 23.3 %all-to-all-start = ((bf16[16,272,128]{2,1,0:T(8,128)(2,1)}), bf16[16,272,128]{2,1,0:T(8,128)(2,1)S(1)}, u32[]{:S(2)}, u32[]{:S(2)}) async-start(bf16[16,272,128]{2,1,0:T(8,128)(2,1)} %shard_map.128), calls=%async_computation | async-start | bytes 2228224 | tf_op jit(solution)/shard_map/all_to_all | solution.py:335
  22.1 0.7 copy-start.8
  82.6 4.6 %copy-start = (bf16[1,2048,256]{2,1,0:T(8,128)(2,1)S(1)}, bf16[1,2048,256]{2,1,0:T(8,128)(2,1)}, u32[]{:S(2)}) copy-start(bf16[1,2048,256]{2,1,0:T(8,128)(2,1)} %param.23) | copy-start | bytes 3145732
  82.6 7.7 %copy-start.1 = (bf16[1,2048,256]{2,1,0:T(8,128)(2,1)S(1)}, bf16[1,2048,256]{2,1,0:T(8,128)(2,1)}, u32[]{:S(2)}) copy-start(bf16[1,2048,256]{2,1,0:T(8,128)(2,1)} %param.24) | copy-start | bytes 3145732
  82.6 63.6 %all-to-all-start.2 = ((bf16[16,512,128]{2,1,0:T(8,128)(2,1)}), bf16[16,512,128]{2,1,0:T(8,128)(2,1)}, u32[]{:S(2)}, u32[]{:S(2)}) async-start(bf16[16,512,128]{2,1,0:T(8,128)(2,1)} %shard_map.131), calls=%async_computation.2 | async-start | bytes 4194304 | tf_op jit(solution)/shard_map/all_to_all | solution.py:335
  87.2 36.4 %collective-permute-start.1 = (bf16[2048,256]{1,0:T(8,128)(2,1)S(1)}, bf16[2048,256]{1,0:T(8,128)(2,1)S(1)}, u32[]{:S(2)}, u32[]{:S(2)}) collective-permute-start(bf16[2048,256]{1,0:T(8,128)(2,1)S(1)} %bitcast.14), channel_id=1, source_target_pairs={{0,1},{1,0},{2,3},{3,2},{4,5},{5,4},{6,7},{7,6},{8,9},{9,8},{10,11... | collective-permute-start | bytes 3145736 | tf_op jit(solution)/shard_map/ppermute | solution.py:345
  90.3 44.5 %collective-permute-start.2 = (bf16[2048,256]{1,0:T(8,128)(2,1)S(1)}, bf16[2048,256]{1,0:T(8,128)(2,1)S(1)}, u32[]{:S(2)}, u32[]{:S(2)}) collective-permute-start(bf16[2048,256]{1,0:T(8,128)(2,1)S(1)} %bitcast.16), channel_id=1, source_target_pairs={{0,1},{1,0},{2,3},{3,2},{4,5},{5,4},{6,7},{7,6},{8,9},{9,8},{10,11... | collective-permute-start | bytes 3145736 | tf_op jit(solution)/shard_map/ppermute | solution.py:345
  92.5 53.7 %collective-permute-start.3 = (bf16[256,2048]{1,0:T(8,128)(2,1)}, bf16[256,2048]{1,0:T(8,128)(2,1)}, u32[]{:S(2)}, u32[]{:S(2)}) collective-permute-start(bf16[256,2048]{1,0:T(8,128)(2,1)} %bitcast.18), channel_id=1, source_target_pairs={{0,1},{1,0},{2,3},{3,2},{4,5},{5,4},{6,7},{7,6},{8,9},{9,8},{10,11... | collective-permute-start | bytes 3145736 | tf_op jit(solution)/shard_map/ppermute | solution.py:345
  123.6 1.0 copy-start.3
  134.8 1.0 copy-start.5
  146.2 1.2 copy-start.2
  147.4 1.2 copy-start.4
  148.6 1.2 copy-start.6
  189.1 30.3 %copy-start.9 = (f32[2,256,128]{2,1,0:T(8,128)S(1)}, f32[2,256,128]{2,1,0:T(8,128)}, u32[]{:S(2)}) copy-start(f32[2,256,128]{2,1,0:T(8,128)} %copy-done.8) | copy-start | bytes 786436

commit v3 on v2

v3 whole, which is shorter than its diff:
```python
import jax
import jax.numpy as jnp
from jax import lax
from jax.experimental import pallas as pl
from jax.experimental.pallas import tpu as pltpu
from jax.sharding import Mesh
from jax.sharding import PartitionSpec as P


TP = ("tp_0", "tp_1")
epsilon = 1e-06
F32 = jnp.float32
BF16 = jnp.bfloat16
HALO = 32
CHUNKS = 1
EXTRA = 16


def vmem(dims, dtype=BF16):
    return pltpu.VMEM(dims, dtype)


def call(kernel, outs, ins, scratch=(), copies=0, spread=False, mib=4, flops=0):
    space = {"h": pltpu.HBM, "v": pltpu.VMEM}
    sems = [pltpu.SemaphoreType.DMA((copies,))] if copies else []
    out_space = pltpu.HBM if spread else pltpu.VMEM
    return pl.pallas_call(
        kernel,
        out_shape=outs,
        in_specs=[pl.BlockSpec(memory_space=space[c]) for c in ins],
        out_specs=jax.tree.map(lambda _: pl.BlockSpec(memory_space=out_space), outs),
        scratch_shapes=list(scratch) + sems,
        cost_estimate=pl.CostEstimate(flops=flops, bytes_accessed=0, transcendentals=0),
        compiler_params=pltpu.CompilerParams(vmem_limit_bytes=mib * 2**20),
    )


def start(pairs, sems, first=0):
    made = [
        pltpu.make_async_copy(src, dst, sems.at[first + i]) for i, (src, dst) in enumerate(pairs)
    ]
    for copy in made:
        copy.start()
    return made


def finish(made):
    for copy in made:
        copy.wait()


def place_of(core, peer):
    return jnp.where(core == 0, peer, (peer % 4) * 4 + peer // 4)


def shape(dims, dtype=BF16):
    return jax.ShapeDtypeStruct(dims, dtype)


def down_lanes(row):
    return jnp.concatenate(
        [
            jnp.transpose(jnp.broadcast_to(row[:, i : i + 128], (128, 128)))
            for i in range(0, row.shape[1], 128)
        ],
        0,
    )


def gate_of(value, gate):
    return (value.astype(F32) * jax.nn.sigmoid(gate.astype(F32))).astype(BF16)


def conv_kernel(halo, gated, docs, consts, sent, gext, dext, out, sems):
    rows, chans = gated.shape
    ntaps = consts.shape[0] - 2
    gext[:HALO] = halo[:HALO].astype(F32)
    gext[HALO:] = gated[...].astype(F32)
    dext[:HALO] = halo[HALO:].astype(F32)
    dext[HALO:] = docs[...].astype(F32)
    kernel = consts[...].astype(F32)
    first = HALO - ntaps + 1
    step = 64
    means = []
    for r in range(0, rows, step):
        doc = dext[HALO + r : HALO + r + step]
        acc = jnp.zeros((step, chans), F32)
        for j in range(ntaps):
            at = first + j + r
            acc = acc + jnp.where(
                dext[at : at + step] == doc, gext[at : at + step] * kernel[j : j + 1], 0.0
            )
        mean = jnp.mean(acc, 1, keepdims=True)
        out[r : r + step] = (acc - mean).astype(BF16)
        means.append(jnp.broadcast_to(mean, (step, 128)))
    lines = []
    for i in range(rows // 128):
        lines.append(jnp.transpose(jnp.concatenate(means[2 * i : 2 * i + 2], 0))[:1])
    mean = jnp.concatenate(lines, 0)
    high = mean.astype(BF16).astype(F32)
    low = mean - high
    tail = jnp.concatenate([high, low, kernel[ntaps:]], 0)
    tail = jnp.concatenate([tail, jnp.zeros((EXTRA - tail.shape[0], 128), F32)], 0)
    out[rows:] = tail.astype(BF16)
    finish(start([(out, sent.at[i]) for i in range(sent.shape[0])], sems))


def routing_kernel(routes, weights, rank_out, pick_out, weight_out):
    rows = routes.shape[1]
    experts = rank_out.shape[0]
    part = 4 * rows // experts // CHUNKS
    expert = lax.broadcasted_iota(jnp.int32, (experts, rows), 0)
    first = routes[:1] == expert
    second = routes[1:] == expert
    named = jnp.logical_or(first, second)
    before = lax.broadcasted_iota(jnp.int32, (rows, rows), 0) < lax.broadcasted_iota(
        jnp.int32, (rows, rows), 1
    )
    rank = jnp.dot(
        named.astype(F32).astype(BF16),
        before.astype(F32).astype(BF16),
        preferred_element_type=F32,
    )
    rank_out[...] = jnp.where(named, rank, -1.0)
    slot = rank + (expert * part).astype(F32)
    for c in range(1, CHUNKS):
        slot = slot + jnp.where(rank >= c * part, float((experts - 1) * part), 0.0)
    for k, chosen in enumerate((first, second)):
        pick = jnp.sum(jnp.where(chosen, slot, 0.0), 0, keepdims=True)
        pick_out[k] = down_lanes(pick)
        weight_out[k] = down_lanes(weights[k : k + 1])


def stream_kernel(parts, out_weight, residual, rank, stream_out, gains, *rest):
    core = lax.axis_index("sp") % 2
    sent, (means, full, act, place) = rest[:CHUNKS], rest[CHUNKS:]
    peers, extended, chans = parts.shape
    rows = extended - EXTRA
    width = peers * chans
    for d in range(peers):
        tail = parts[place_of(core, d), rows:].astype(F32)
        gains[d : d + 1] = tail[2 * (rows // 128) + 1 : 2 * (rows // 128) + 2]
        for i in range(rows // 128):
            means[d : d + 1, 128 * i : 128 * (i + 1)] = tail[i : i + 1]
            means[peers + d : peers + d + 1, 128 * i : 128 * (i + 1)] = tail[
                rows // 128 + i : rows // 128 + i + 1
            ]
    owner = lax.broadcasted_iota(jnp.int32, (2 * peers, width), 0)
    block = lax.broadcasted_iota(jnp.int32, (2 * peers, width), 1) // chans
    spread = jnp.logical_or(owner == block, owner == block + peers).astype(F32).astype(BF16)
    full[...] = lax.dot_general(
        means[...].astype(BF16),
        spread,
        (((0,), (0,)), ((), ())),
        preferred_element_type=F32,
    )
    nextra = 2 * (rows // 128)
    step = 64
    for r in range(0, rows, step):
        total = jnp.zeros((step, chans), F32)
        square = jnp.zeros((step, chans), F32)
        for d in range(peers):
            x = full[r : r + step, d * chans : (d + 1) * chans] + parts[
                place_of(core, d), r : r + step
            ].astype(F32)
            full[r : r + step, d * chans : (d + 1) * chans] = x
            total = total + x
            square = square + x * x
        mean = jnp.sum(total, 1, keepdims=True) / width
        var = jnp.sum(square, 1, keepdims=True) / width - mean * mean
        scale = lax.rsqrt(var + epsilon)
        for d in range(peers):
            gain = parts[place_of(core, d), rows:].astype(F32)[nextra : nextra + 1]
            x = full[r : r + step, d * chans : (d + 1) * chans]
            x = (x - mean) * scale * gain
            act[r : r + step, d * chans : (d + 1) * chans] = (x / (1.0 + jnp.exp(-x))).astype(BF16)
    projected = jnp.dot(act[...], out_weight[...], preferred_element_type=F32).astype(BF16)
    stream = (residual[...].astype(F32) + projected.astype(F32)).astype(BF16)
    stream_out[...] = stream
    experts, part, _ = sent[0].shape
    slots = experts * part
    slot = lax.broadcasted_iota(jnp.int32, (part, rows), 0)
    for c in range(CHUNKS):
        wanted = (slot + c * part).astype(F32)
        for e in range(experts):
            at = c * slots + e * part
            place[at : at + part] = (rank[e : e + 1] == wanted).astype(F32).astype(BF16)
    moved = jnp.dot(place[...], stream, preferred_element_type=F32).astype(BF16)
    for c in range(CHUNKS):
        sent[c][...] = moved[c * slots : (c + 1) * slots].reshape(sent[c].shape)


def expert_kernel(
    parts,
    gains,
    gate_ah,
    up_ah,
    down_ah,
    gate_bh,
    up_bh,
    down_bh,
    out,
    normed,
    gate_a,
    up_a,
    down_a,
    gate_b,
    up_b,
    down_b,
    sems,
):
    made = start(
        [
            (gate_ah, gate_a),
            (up_ah, up_a),
            (gate_bh, gate_b),
            (up_bh, up_b),
            (down_ah, down_a),
            (down_bh, down_b),
        ],
        sems,
    )
    core = lax.axis_index("sp") % 2
    peers, rows, chans = parts.shape
    width = peers * chans
    step = 64
    for r in range(0, rows, step):
        square = jnp.zeros((step, chans), F32)
        for d in range(peers):
            x = parts[d, r : r + step].astype(F32)
            square = square + x * x
        scale = lax.rsqrt(jnp.sum(square, 1, keepdims=True) / width + epsilon)
        for d in range(peers):
            x = parts[place_of(core, d), r : r + step].astype(F32) * scale * gains[d : d + 1]
            normed[r : r + step, d * chans : (d + 1) * chans] = x.astype(BF16)
    finish(made)
    step = 256
    for r in range(0, rows, step):
        x = normed[r : r + step]
        hidden = []
        for gate_w, up_w in ((gate_a, up_a), (gate_b, up_b)):
            gate = jnp.dot(x, gate_w[...], preferred_element_type=F32)
            up = jnp.dot(x, up_w[...], preferred_element_type=F32)
            hidden.append((gate / (1.0 + jnp.exp(-gate)) * up).astype(BF16))
        for c in range(0, width, 512):
            y = jnp.dot(hidden[0], down_a[:, c : c + 512], preferred_element_type=F32)
            y = y + jnp.dot(hidden[1], down_b[:, c : c + 512], preferred_element_type=F32)
            y = y.astype(BF16)
            for i in range(512 // chans):
                out[place_of(core, c // chans + i), r : r + step] = y[:, i * chans : (i + 1) * chans]


def mix_kernel(*refs):
    returned, (pick, weight, stream, out) = refs[:CHUNKS], refs[CHUNKS:]
    rows = stream.shape[0]
    slots = returned[0].shape[0]
    lane = lax.broadcasted_iota(jnp.int32, (rows, 128), 1).astype(F32)
    routed = jnp.zeros(stream.shape, F32)
    for k in range(2):
        picked = jnp.zeros(stream.shape, F32)
        for c in range(CHUNKS):
            choose = jnp.concatenate(
                [
                    (pick[k] == lane + float(c * slots + s)).astype(F32).astype(BF16)
                    for s in range(0, slots, 128)
                ],
                1,
            )
            picked = picked + jnp.dot(choose, returned[c][...], preferred_element_type=F32)
        routed = routed + picked * weight[k]
    out[...] = (stream[...].astype(F32) + routed).astype(BF16)


def exchange(x, axis):
    return lax.all_to_all(x, axis, split_axis=0, concat_axis=0, tiled=True)


def rings(first):
    groups = []
    for s in range(lax.axis_size("sp")):
        along_x = (s % 2 == 0) == first
        for a in range(4):
            groups.append([s * 16 + (4 * a + b if along_x else 4 * b + a) for b in range(4)])
    return groups


def ring_exchange(x, first):
    return lax.all_to_all(
        x, ("sp", *TP), split_axis=0, concat_axis=0, axis_index_groups=rings(first), tiled=True
    )


def four_copies(x):
    return jnp.broadcast_to(x, (4, *x.shape))


def swap_pair(x):
    groups, peers = lax.axis_size("sp"), lax.axis_size(TP)
    pairs = [
        (s * peers + t, s * peers + (t ^ (1 if s % 2 == 0 else 4)))
        for s in range(groups)
        for t in range(peers)
    ]
    return lax.ppermute(x, ("sp", *TP), pairs)


def per_device(
    residual_in,
    conv_value,
    conv_gate,
    doc_ids,
    conv_kernel_w,
    ln_gain,
    out_weight,
    norm_gain,
    routes,
    route_weight,
    gate_w,
    up_w,
    down_w,
):
    rows, chans = conv_value.shape
    experts = lax.axis_size("sp")
    peers = lax.axis_size(TP)
    capacity = 4 * rows // experts
    slots = experts * capacity
    width = peers * chans
    gate_a, up_a, down_a = gate_w[0], up_w[0], down_w[0]

    gated = gate_of(conv_value, conv_gate)
    docs = jnp.broadcast_to(doc_ids.astype(BF16)[:, None], (rows, chans))
    consts = jnp.concatenate([conv_kernel_w, ln_gain[None], norm_gain[None]], 0)
    tail = jnp.concatenate(
        [
            gate_of(conv_value[rows - HALO :], conv_gate[rows - HALO :]),
            jnp.broadcast_to(doc_ids[rows - HALO :].astype(BF16)[:, None], (HALO, chans)),
        ],
        0,
    )
    n = lax.axis_size("sp")
    halo = lax.ppermute(tail, "sp", [(i, i + 1) for i in range(n - 1)])
    gate_b = swap_pair(gate_a)
    up_b = swap_pair(up_a)
    down_b = swap_pair(down_a)
    packed = call(
        conv_kernel,
        shape((4, rows + EXTRA, chans)),
        "vvvv",
        [
            vmem((rows + HALO, chans), F32),
            vmem((rows + HALO, chans), F32),
            vmem((rows + EXTRA, chans)),
        ],
        copies=4,
        spread=True,
    )(halo, gated, docs, consts)
    rank, pick, weight = call(
        routing_kernel,
        (shape((experts, rows), F32), shape((2, rows, 128), F32), shape((2, rows, 128), F32)),
        "vv",
    )(routes.T, route_weight.T)
    parts = ring_exchange(packed, True)
    parts = ring_exchange(four_copies(parts), False).reshape(peers, rows + EXTRA, chans)
    part = capacity // CHUNKS
    stream, gains, *sent = call(
        stream_kernel,
        (shape((rows, chans)), shape((peers, chans), F32)) + (shape((experts, part, chans)),) * CHUNKS,
        "vvvv",
        [
            vmem((2 * peers, rows), F32),
            vmem((rows, width), F32),
            vmem((rows, width)),
            vmem((slots, rows)),
        ],
        mib=16,
    )(parts, out_weight, residual_in, rank)
    half = slots // CHUNKS // 2
    returned = []
    for c in range(CHUNKS):
        received = exchange(sent[c], "sp")
        halves = received.reshape(1, 2, half, chans)
        outbound = jnp.broadcast_to(halves, (2, 2, half, chans)).reshape(4, half, chans)
        gathered = ring_exchange(outbound, True)
        gathered = ring_exchange(four_copies(gathered), False).reshape(peers, half, chans)
        partial = call(
            expert_kernel,
            shape((peers, half, chans)),
            "vvhhhhhh",
            [vmem((half, width))]
            + [vmem(gate_a.shape), vmem(up_a.shape), vmem(down_a.shape)] * 2,
            copies=6,
            mib=20,
        )(gathered, gains, gate_a, up_a, down_a, gate_b, up_b, down_b)
        pieces = ring_exchange(partial.reshape(4, 4, half, chans), False)
        summed = jnp.sum(pieces.astype(F32), 0).astype(BF16)
        pieces = ring_exchange(summed, True).reshape(2, 2, half, chans)
        summed = jnp.sum(pieces.astype(F32), 0).astype(BF16)
        back = exchange(summed.reshape(experts, part, chans), "sp")
        returned.append(back.reshape(2 * half, chans))
    return call(mix_kernel, shape((rows, chans)), "v" * (CHUNKS + 3))(
        *returned, pick, weight, stream
    )


def solution(mesh):
    split = Mesh(mesh.devices.reshape(mesh.shape["sp"], 4, 4), ("sp", "tp_0", "tp_1"))
    in_specs = (
        P("sp", TP),
        P("sp", TP),
        P("sp", TP),
        P("sp"),
        P(None, TP),
        P(TP),
        P(None, TP),
        P(TP),
        P("sp", None),
        P("sp", None),
        P("sp", None, TP),
        P("sp", None, TP),
        P("sp", TP, None),
    )
    out_specs = P("sp", TP)
    return jax.shard_map(
        per_device, mesh=split, in_specs=in_specs, out_specs=out_specs, check_vma=False
    )
```

time: 221 us -> 211 us (0.955)
  waiting for transfers between devices: 70.9 us -> 51 us
  blocking collectives: 98.2 us -> 112 us
  Pallas kernels: 16.5 us -> 9.56 us
  other arithmetic: 0 us -> 3.92 us
    all_to_all x0 -> x4, blocking collectives: none -> 45.4 us  [ring_exchange(): lax.all_to_all(x, ('sp', *TP), split_axis=0, concat_axis=0, axis_index_gr...]
    all_to_all x3 -> x2, blocking collectives: 98.2 us -> 67 us  [exchange(): return lax.all_to_all(x, axis, split_axis=0, concat_axis=0, tiled=True)]
    all_to_all x2, waiting for transfers between devices: 18.5 us -> 9.27 us  [ring_exchange(): lax.all_to_all(x, ('sp', *TP), split_axis=0, concat_axis=0, axis_index_gr...]
    ppermute x3, waiting for transfers between devices: 48.6 us -> 39.5 us  [swap_pair(): return lax.ppermute(x, ('sp', *TP), pairs)]
    pallas_call x1, Pallas kernels: 8.89 us -> 4.88 us  [per_device(): call(expert_kernel, shape((peers, half, chans)), 'vvhhhhhh', [vmem((half,...]
    unnamed x45 -> x30, local copies, waits for them, and re-layouts: 13.1 us -> 9.8 us
    broadcast_in_dim x0 -> x4, local copies, waits for them, and re-layouts: none -> 3.07 us  [the longest x2 2.91 us: four_copies(): return jnp.broadcast_to(x, (4, *x.shape))]
    pallas_call x6 -> x3, Pallas kernels: 7.25 us -> 4.34 us  [the longest x1 2.09 us: per_device(): call(stream_kernel, (shape((rows, chans)), shape((peers, chans), F32)) +...]
  transfers between devices with their start and end apart: 6 -> 6, of which waited for: 5 -> 5; matrix products, arithmetic and copies ran while one was open for 0% -> 1% of each run, Pallas kernels for 0% -> 0%
where the time goes in v3:
time: 211 us; the launch traced here: 210 us
  blocking collectives  112 us (53%)
  waiting for transfers between devices  51 us (24%)
  starting transfers between devices  19.9 us (9%)
  local copies, waits for them, and re-layouts  13 us (6%)
  Pallas kernels  9.56 us (5%)
  other arithmetic  3.92 us (2%)
    all_to_all x2, blocking collectives, exchange(): return lax.all_to_all(x, axis, split_axis=0, concat_axis=0, tiled=True)  67 us
    all_to_all x4, blocking collectives, ring_exchange(): lax.all_to_all(x, ('sp', *TP), split_axis=0, concat_axis=0, axis_index_gr...  45.4 us
    ppermute x3, waiting for transfers between devices, swap_pair(): return lax.ppermute(x, ('sp', *TP), pairs)  39.5 us
    unnamed x30, local copies, waits for them, and re-layouts  9.8 us
    all_to_all x2, waiting for transfers between devices, ring_exchange(): lax.all_to_all(x, ('sp', *TP), split_axis=0, concat_axis=0, axis_index_gr...  9.27 us
    ppermute x3, starting transfers between devices, swap_pair(): return lax.ppermute(x, ('sp', *TP), pairs)  7.77 us
    all_to_all x2, starting transfers between devices, ring_exchange(): lax.all_to_all(x, ('sp', *TP), split_axis=0, concat_axis=0, axis_index_gr...  7.26 us
    ppermute x1, starting transfers between devices, per_device(): halo = lax.ppermute(tail, 'sp', [(i, i + 1) for i in range(n - 1)])  4.92 us
  transfers between devices with their start and end apart: 6, of which 5 were waited for; matrix products, arithmetic and copies ran while one was open for 1% of the time, Pallas kernels for 0%

profile of v3, /device:TPU:1, one launch (start us, length us, event | category | flops | bytes accessed | tf_op | source)
XLA Modules:
  0.0 210.1 jit_solution(8070143920538089024)
XLA Ops:
  0.0 0.7 convert.5
  0.7 0.1 slice.12
  0.8 0.1 pad.4.clone
  0.8 0.7 multiply_convert_fusion.1
  1.6 0.1 pad_maximum_fusion
  1.6 4.9 %collective-permute-start = (bf16[64,128]{1,0:T(8,128)(2,1)S(1)}, bf16[64,128]{1,0:T(8,128)(2,1)S(1)}, u32[]{:S(2)}, u32[]{:S(2)}) collective-permute-start(bf16[64,128]{1,0:T(8,128)(2,1)S(1)} %pad_maximum_fusion), channel_id=1, source_target_pairs={{0,16},{16,32},{32,48},{48,64},{64,80},{80,96},{96,112},{112,128},... | collective-permute-start | bytes 49160 | tf_op jit(solution)/shard_map/ppermute | solution.py:341
  6.6 0.9 multiply_convert_fusion.gated
  7.5 0.7 pad_maximum_fusion.1.consts
  8.2 2.2 %collective-permute-done.halo = bf16[64,128]{1,0:T(8,128)(2,1)S(1)} collective-permute-done((bf16[64,128]{1,0:T(8,128)(2,1)S(1)}, bf16[64,128]{1,0:T(8,128)(2,1)S(1)}, u32[]{:S(2)}, u32[]{:S(2)}) %collective-permute-start) | collective-permute-done | bytes 16416 | tf_op jit(solution)/shard_map/ppermute | solution.py:341
  10.4 0.1 broadcast_in_dim.32.docs
  10.5 1.1 shard_map.127
  11.7 0.0 copy-start.13
  11.7 0.0 copy-start.14
  11.7 0.0 copy-start.9
  11.7 0.0 copy-start.12
  11.7 8.1 %all_to_all.40 = bf16[4,272,128]{2,1,0:T(8,128)(2,1)S(1)} all-to-all(bf16[4,272,128]{2,1,0:T(8,128)(2,1)S(1)} %shard_map.127), channel_id=1, replica_groups={{0,1,2,3},{4,5,6,7},{8,9,10,11},{12,13,14,15},{16,20,24,28},{17,21,25,2..., dimensions={0} | all-to-all | bytes 557056 | tf_op jit(solution)/shard_map/all_to_all | solution.py:288
  19.8 1.2 broadcast_in_dim.35
  21.0 3.5 %all-to-all-start.1 = ((bf16[4,4,272,128]{3,2,1,0:T(8,128)(2,1)}), bf16[4,4,272,128]{3,2,1,0:T(8,128)(2,1)S(1)}, u32[]{:S(2)}, u32[]{:S(2)}) async-start(bf16[4,4,272,128]{3,2,1,0:T(8,128)(2,1)} %broadcast_in_dim.35), calls=%async_computation.1 | async-start | bytes 2228224 | tf_op jit(solution)/shard_map/all_to_all | solution.py:288
  24.5 0.3 shard_map.128
  24.9 0.7 copy-done.10
  25.6 9.3 %all-to-all-done.1 = bf16[4,4,272,128]{3,2,1,0:T(8,128)(2,1)S(1)} async-done(((bf16[4,4,272,128]{3,2,1,0:T(8,128)(2,1)}), bf16[4,4,272,128]{3,2,1,0:T(8,128)(2,1)S(1)}, u32[]{:S(2)}, u32[]{:S(2)}) %all-to-all-start.1) | async-done | bytes 1114144 | tf_op jit(solution)/shard_map/all_to_all | solution.py:288
  34.9 2.1 shard_map.129
  37.0 41.0 %all_to_all.41 = bf16[32,32,128]{2,1,0:T(8,128)(2,1)S(1)} all-to-all(bf16[32,32,128]{2,1,0:T(8,128)(2,1)S(1)} %get-tuple-element.12), channel_id=1, replica_groups=mesh['sp'=32,'tp_0'=4,'tp_1'=4] {'sp'}, dimensions={0} | all-to-all | bytes 524288 | tf_op jit(solution)/shard_map/all_to_all | solution.py:275
  77.9 0.1 broadcast_in_dim.37
  78.0 9.3 %all_to_all.42 = bf16[4,512,128]{2,1,0:T(8,128)(2,1)S(1)} all-to-all(bf16[4,512,128]{2,1,0:T(8,128)(2,1)S(1)} %bitcast.28), channel_id=1, replica_groups={{0,1,2,3},{4,5,6,7},{8,9,10,11},{12,13,14,15},{16,20,24,28},{17,21,25,2..., dimensions={0} | all-to-all | bytes 1048576 | tf_op jit(solution)/shard_map/all_to_all | solution.py:288
  87.4 1.7 broadcast_in_dim.38
  89.1 3.7 %all-to-all-start.4 = ((bf16[4,4,512,128]{3,2,1,0:T(8,128)(2,1)}), bf16[4,4,512,128]{3,2,1,0:T(8,128)(2,1)S(1)}, u32[]{:S(2)}, u32[]{:S(2)}) async-start(bf16[4,4,512,128]{3,2,1,0:T(8,128)(2,1)} %broadcast_in_dim.38), calls=%async_computation.4 | async-start | bytes 4194304 | tf_op jit(solution)/shard_map/all_to_all | solution.py:288
  92.9 2.5 %collective-permute-start.1 = (bf16[2048,256]{1,0:T(8,128)(2,1)S(1)}, bf16[2048,256]{1,0:T(8,128)(2,1)S(1)}, u32[]{:S(2)}, u32[]{:S(2)}) collective-permute-start(bf16[2048,256]{1,0:T(8,128)(2,1)S(1)} %bitcast.18), channel_id=1, source_target_pairs={{0,1},{1,0},{2,3},{3,2},{4,5},{5,4},{6,7},{7,6},{8,9},{9,8},{10,11... | collective-permute-start | bytes 3145736 | tf_op jit(solution)/shard_map/ppermute | solution.py:304
  95.4 2.8 %collective-permute-start.2 = (bf16[2048,256]{1,0:T(8,128)(2,1)}, bf16[2048,256]{1,0:T(8,128)(2,1)S(1)}, u32[]{:S(2)}, u32[]{:S(2)}) collective-permute-start(bf16[2048,256]{1,0:T(8,128)(2,1)} %bitcast.20), channel_id=1, source_target_pairs={{0,1},{1,0},{2,3},{3,2},{4,5},{5,4},{6,7},{7,6},{8,9},{9,8},{10,11... | collective-permute-start | bytes 3145736 | tf_op jit(solution)/shard_map/ppermute | solution.py:304
  98.2 2.5 %collective-permute-start.3 = (bf16[256,2048]{1,0:T(8,128)(2,1)}, bf16[256,2048]{1,0:T(8,128)(2,1)S(1)}, u32[]{:S(2)}, u32[]{:S(2)}) collective-permute-start(bf16[256,2048]{1,0:T(8,128)(2,1)} %bitcast.22), channel_id=1, source_target_pairs={{0,1},{1,0},{2,3},{3,2},{4,5},{5,4},{6,7},{7,6},{8,9},{9,8},{10,11... | collective-permute-start | bytes 3145736 | tf_op jit(solution)/shard_map/ppermute | solution.py:304
  100.7 18.8 %collective-permute-done.1.gate_bh = bf16[2048,256]{1,0:T(8,128)(2,1)S(1)} collective-permute-done((bf16[2048,256]{1,0:T(8,128)(2,1)S(1)}, bf16[2048,256]{1,0:T(8,128)(2,1)S(1)}, u32[]{:S(2)}, u32[]{:S(2)}) %collective-permute-start.1) | collective-permute-done | bytes 1048608 | tf_op jit(solution)/shard_map/ppermute | solution.py:304
  119.4 1.0 copy-done.3
  120.4 10.8 %collective-permute-done.2.up_bh = bf16[2048,256]{1,0:T(8,128)(2,1)S(1)} collective-permute-done((bf16[2048,256]{1,0:T(8,128)(2,1)}, bf16[2048,256]{1,0:T(8,128)(2,1)S(1)}, u32[]{:S(2)}, u32[]{:S(2)}) %collective-permute-start.2) | collective-permute-done | bytes 1048608 | tf_op jit(solution)/shard_map/ppermute | solution.py:304
  131.2 1.0 copy-done.5
  132.2 9.9 %collective-permute-done.3.down_bh = bf16[256,2048]{1,0:T(8,128)(2,1)S(1)} collective-permute-done((bf16[256,2048]{1,0:T(8,128)(2,1)}, bf16[256,2048]{1,0:T(8,128)(2,1)S(1)}, u32[]{:S(2)}, u32[]{:S(2)}) %collective-permute-start.3) | collective-permute-done | bytes 1048608 | tf_op jit(solution)/shard_map/ppermute | solution.py:304
  142.1 1.0 copy-done.7
  143.1 1.2 copy-done.1
  144.3 1.2 copy-done.2
  145.5 1.2 copy-done.4
  146.8 1.2 copy-done.6
  148.0 1.2 copy-done.8
  149.2 4.9 %shard_map.130 = bf16[16,512,128]{2,1,0:T(8,128)(2,1)S(1)} custom-call(bf16[16,512,128]{2,1,0:T(8,128)(2,1)S(1)} %bitcast.15, f32[16,128]{1,0:T(8,128)S(1)} %get-tuple-element.13.gains, bf16[2048,256]{1,0:T(8,128)(2,1)S(1)} %bitcast.19, bf16[2048,256]{1,0:T(8,128)(2,1)S(1)} %bitcast.21, bf16[256,2048]{1,0:T(8,128)(2,1)S(1)} %bitcast.23, ...), custom_call_target="tpu_custom_call" | custom-call | tf_op jit(solution)/shard_map/pallas_call | solution.py:385
  154.1 17.8 %all_to_all.43 = bf16[4,4,512,128]{3,2,1,0:T(8,128)(2,1)S(1)} all-to-all(bf16[4,4,512,128]{3,2,1,0:T(8,128)(2,1)S(1)} %bitcast.16), channel_id=1, replica_groups={{0,4,8,12},{1,5,9,13},{2,6,10,14},{3,7,11,15},{16,17,18,19},{20,21,22,2..., dimensions={0} | all-to-all | bytes 4194304 | tf_op jit(solution)/shard_map/all_to_all | solution.py:288
  172.0 0.6 reduce_sum.24
  172.5 10.1 %all_to_all.44 = bf16[4,512,128]{2,1,0:T(8,128)(2,1)S(1)} all-to-all(bf16[4,512,128]{2,1,0:T(8,128)(2,1)S(1)} %reduce_sum.24), channel_id=1, replica_groups={{0,1,2,3},{4,5,6,7},{8,9,10,11},{12,13,14,15},{16,20,24,28},{17,21,25,2..., dimensions={0} | all-to-all | bytes 1048576 | tf_op jit(solution)/shard_map/all_to_all | solution.py:288
  182.7 0.2 reduce_sum.25
  182.9 26.1 %all_to_all.45 = bf16[32,32,128]{2,1,0:T(8,128)(2,1)S(1)} all-to-all(bf16[32,32,128]{2,1,0:T(8,128)(2,1)S(1)} %bitcast.30), channel_id=1, replica_groups=mesh['sp'=32,'tp_0'=4,'tp_1'=4] {'sp'}, dimensions={0} | all-to-all | bytes 524288 | tf_op jit(solution)/shard_map/all_to_all | solution.py:275
  208.9 1.1 shard_map.131
  (18 shorter events, 0.0 us)
Async XLA Ops:
  1.6 8.8 %collective-permute-start = (bf16[64,128]{1,0:T(8,128)(2,1)S(1)}, bf16[64,128]{1,0:T(8,128)(2,1)S(1)}, u32[]{:S(2)}, u32[]{:S(2)}) collective-permute-start(bf16[64,128]{1,0:T(8,128)(2,1)S(1)} %pad_maximum_fusion), channel_id=1, source_target_pairs={{0,16},{16,32},{32,48},{48,64},{64,80},{80,96},{96,112},{112,128},... | collective-permute-start | bytes 49160 | tf_op jit(solution)/shard_map/ppermute | solution.py:341
  11.7 12.8 %copy-start.13 = (s32[256,2]{0,1:T(2,128)S(1)}, s32[256,2]{0,1:T(2,128)}, u32[]{:S(2)}) copy-start(s32[256,2]{0,1:T(2,128)} %param.21) | copy-start | bytes 6148
  11.7 12.8 %copy-start.14 = (f32[256,2]{0,1:T(2,128)S(1)}, f32[256,2]{0,1:T(2,128)}, u32[]{:S(2)}) copy-start(f32[256,2]{0,1:T(2,128)} %param.22) | copy-start | bytes 6148
  11.7 23.2 %copy-start.9 = (bf16[2048,128]{1,0:T(8,128)(2,1)S(1)}, bf16[2048,128]{1,0:T(8,128)(2,1)}, u32[]{:S(2)}) copy-start(bf16[2048,128]{1,0:T(8,128)(2,1)} %out_weight.1) | copy-start | bytes 1572868
  11.7 23.2 %copy-start.12 = (bf16[256,128]{1,0:T(8,128)(2,1)S(1)}, bf16[256,128]{1,0:T(8,128)(2,1)}, u32[]{:S(2)}) copy-start(bf16[256,128]{1,0:T(8,128)(2,1)} %residual.1) | copy-start | bytes 196612
  21.0 13.9 %all-to-all-start.1 = ((bf16[4,4,272,128]{3,2,1,0:T(8,128)(2,1)}), bf16[4,4,272,128]{3,2,1,0:T(8,128)(2,1)S(1)}, u32[]{:S(2)}, u32[]{:S(2)}) async-start(bf16[4,4,272,128]{3,2,1,0:T(8,128)(2,1)} %broadcast_in_dim.35), calls=%async_computation.1 | async-start | bytes 2228224 | tf_op jit(solution)/shard_map/all_to_all | solution.py:288
  24.9 0.7 copy-start.10
  89.1 3.8 %copy-start = (bf16[1,2048,256]{2,1,0:T(8,128)(2,1)S(1)}, bf16[1,2048,256]{2,1,0:T(8,128)(2,1)}, u32[]{:S(2)}) copy-start(bf16[1,2048,256]{2,1,0:T(8,128)(2,1)} %param.23) | copy-start | bytes 3145732
  89.1 54.0 %all-to-all-start.4 = ((bf16[4,4,512,128]{3,2,1,0:T(8,128)(2,1)}), bf16[4,4,512,128]{3,2,1,0:T(8,128)(2,1)S(1)}, u32[]{:S(2)}, u32[]{:S(2)}) async-start(bf16[4,4,512,128]{3,2,1,0:T(8,128)(2,1)} %broadcast_in_dim.38), calls=%async_computation.4 | async-start | bytes 4194304 | tf_op jit(solution)/shard_map/all_to_all | solution.py:288
  92.9 26.5 %collective-permute-start.1 = (bf16[2048,256]{1,0:T(8,128)(2,1)S(1)}, bf16[2048,256]{1,0:T(8,128)(2,1)S(1)}, u32[]{:S(2)}, u32[]{:S(2)}) collective-permute-start(bf16[2048,256]{1,0:T(8,128)(2,1)S(1)} %bitcast.18), channel_id=1, source_target_pairs={{0,1},{1,0},{2,3},{3,2},{4,5},{5,4},{6,7},{7,6},{8,9},{9,8},{10,11... | collective-permute-start | bytes 3145736 | tf_op jit(solution)/shard_map/ppermute | solution.py:304
  95.4 35.8 %collective-permute-start.2 = (bf16[2048,256]{1,0:T(8,128)(2,1)}, bf16[2048,256]{1,0:T(8,128)(2,1)S(1)}, u32[]{:S(2)}, u32[]{:S(2)}) collective-permute-start(bf16[2048,256]{1,0:T(8,128)(2,1)} %bitcast.20), channel_id=1, source_target_pairs={{0,1},{1,0},{2,3},{3,2},{4,5},{5,4},{6,7},{7,6},{8,9},{9,8},{10,11... | collective-permute-start | bytes 3145736 | tf_op jit(solution)/shard_map/ppermute | solution.py:304
  98.2 43.9 %collective-permute-start.3 = (bf16[256,2048]{1,0:T(8,128)(2,1)}, bf16[256,2048]{1,0:T(8,128)(2,1)S(1)}, u32[]{:S(2)}, u32[]{:S(2)}) collective-permute-start(bf16[256,2048]{1,0:T(8,128)(2,1)} %bitcast.22), channel_id=1, source_target_pairs={{0,1},{1,0},{2,3},{3,2},{4,5},{5,4},{6,7},{7,6},{8,9},{9,8},{10,11... | collective-permute-start | bytes 3145736 | tf_op jit(solution)/shard_map/ppermute | solution.py:304
  119.4 1.0 copy-start.3
  131.2 1.0 copy-start.5
  142.1 1.0 copy-start.7
  143.1 1.2 copy-start.1
  144.3 1.2 copy-start.2
  145.5 1.2 copy-start.4
  146.8 1.2 copy-start.6
  148.0 1.2 copy-start.8
  172.0 37.0 %copy-start.11 = (f32[2,256,128]{2,1,0:T(8,128)S(1)}, f32[2,256,128]{2,1,0:T(8,128)}, u32[]{:S(2)}) copy-start(f32[2,256,128]{2,1,0:T(8,128)} %copy-done.10) | copy-start | bytes 786436

commit v4 on v3

--- a/solution.py
+++ b/solution.py
@@ -132,13 +132,12 @@
 
 
 def stream_kernel(parts, out_weight, residual, rank, stream_out, gains, *rest):
-    core = lax.axis_index("sp") % 2
     sent, (means, full, act, place) = rest[:CHUNKS], rest[CHUNKS:]
     peers, extended, chans = parts.shape
     rows = extended - EXTRA
     width = peers * chans
     for d in range(peers):
-        tail = parts[place_of(core, d), rows:].astype(F32)
+        tail = parts[d, rows:].astype(F32)
         gains[d : d + 1] = tail[2 * (rows // 128) + 1 : 2 * (rows // 128) + 2]
         for i in range(rows // 128):
             means[d : d + 1, 128 * i : 128 * (i + 1)] = tail[i : i + 1]
@@ -161,7 +160,7 @@
         square = jnp.zeros((step, chans), F32)
         for d in range(peers):
             x = full[r : r + step, d * chans : (d + 1) * chans] + parts[
-                place_of(core, d), r : r + step
+                d, r : r + step
             ].astype(F32)
             full[r : r + step, d * chans : (d + 1) * chans] = x
             total = total + x
@@ -170,7 +169,7 @@
         var = jnp.sum(square, 1, keepdims=True) / width - mean * mean
         scale = lax.rsqrt(var + epsilon)
         for d in range(peers):
-            gain = parts[place_of(core, d), rows:].astype(F32)[nextra : nextra + 1]
+            gain = parts[d, rows:].astype(F32)[nextra : nextra + 1]
             x = full[r : r + step, d * chans : (d + 1) * chans]
             x = (x - mean) * scale * gain
             act[r : r + step, d * chans : (d + 1) * chans] = (x / (1.0 + jnp.exp(-x))).astype(BF16)
@@ -344,14 +343,14 @@
     down_b = swap_pair(down_a)
     packed = call(
         conv_kernel,
-        shape((4, rows + EXTRA, chans)),
+        shape((peers, rows + EXTRA, chans)),
         "vvvv",
         [
             vmem((rows + HALO, chans), F32),
             vmem((rows + HALO, chans), F32),
             vmem((rows + EXTRA, chans)),
         ],
-        copies=4,
+        copies=peers,
         spread=True,
     )(halo, gated, docs, consts)
     rank, pick, weight = call(
@@ -359,8 +358,7 @@
         (shape((experts, rows), F32), shape((2, rows, 128), F32), shape((2, rows, 128), F32)),
         "vv",
     )(routes.T, route_weight.T)
-    parts = ring_exchange(packed, True)
-    parts = ring_exchange(four_copies(parts), False).reshape(peers, rows + EXTRA, chans)
+    parts = exchange(packed, TP)
     part = capacity // CHUNKS
     stream, gains, *sent = call(
         stream_kernel,

time: 211 us -> 208 us (0.986)
  blocking collectives: 112 us -> 99.6 us
  waiting for transfers between devices: 51 us -> 60.1 us
    all_to_all x0 -> x1, waiting for transfers between devices: none -> 18.4 us  [exchange(): return lax.all_to_all(x, axis, split_axis=0, concat_axis=0, tiled=True)]
    all_to_all x2 -> x1, waiting for transfers between devices: 9.27 us -> 0.01 us  [ring_exchange(): lax.all_to_all(x, ('sp', *TP), split_axis=0, concat_axis=0, axis_index_gr...]
    all_to_all x4 -> x3, blocking collectives: 45.4 us -> 37.3 us  [ring_exchange(): lax.all_to_all(x, ('sp', *TP), split_axis=0, concat_axis=0, axis_index_gr...]
    all_to_all x2, blocking collectives: 67 us -> 62.3 us  [exchange(): return lax.all_to_all(x, axis, split_axis=0, concat_axis=0, tiled=True)]
    all_to_all x0 -> x1, starting transfers between devices: none -> 4.59 us  [exchange(): return lax.all_to_all(x, axis, split_axis=0, concat_axis=0, tiled=True)]
    all_to_all x2 -> x1, starting transfers between devices: 7.26 us -> 3.74 us  [ring_exchange(): lax.all_to_all(x, ('sp', *TP), split_axis=0, concat_axis=0, axis_index_gr...]
where the time goes in v4:
time: 208 us; the launch traced here: 207 us
  blocking collectives  99.6 us (48%)
  waiting for transfers between devices  60.1 us (29%)
  starting transfers between devices  21 us (10%)
  local copies, waits for them, and re-layouts  11.9 us (6%)
  Pallas kernels  10.3 us (5%)
  other arithmetic  3.98 us (2%)
    all_to_all x2, blocking collectives, exchange(): return lax.all_to_all(x, axis, split_axis=0, concat_axis=0, tiled=True)  62.3 us
    ppermute x3, waiting for transfers between devices, swap_pair(): return lax.ppermute(x, ('sp', *TP), pairs)  39.5 us
    all_to_all x3, blocking collectives, ring_exchange(): lax.all_to_all(x, ('sp', *TP), split_axis=0, concat_axis=0, axis_index_gr...  37.3 us
    all_to_all x1, waiting for transfers between devices, exchange(): return lax.all_to_all(x, axis, split_axis=0, concat_axis=0, tiled=True)  18.4 us
    unnamed x30, local copies, waits for them, and re-layouts  9.79 us
    ppermute x3, starting transfers between devices, swap_pair(): return lax.ppermute(x, ('sp', *TP), pairs)  7.77 us
    ppermute x1, starting transfers between devices, per_device(): halo = lax.ppermute(tail, 'sp', [(i, i + 1) for i in range(n - 1)])  4.92 us
    pallas_call x1, Pallas kernels, per_device(): call(expert_kernel, shape((peers, half, chans)), 'vvhhhhhh', [vmem((half,...  4.88 us
  transfers between devices with their start and end apart: 6, of which 5 were waited for; matrix products, arithmetic and copies ran while one was open for 1% of the time, Pallas kernels for 0%

profile of v4, /device:TPU:1, one launch (start us, length us, event | category | flops | bytes accessed | tf_op | source)
XLA Modules:
  0.0 206.9 jit_solution(1568798961393183456)
XLA Ops:
  0.0 0.0 copy-start.9
  0.0 0.7 convert.5
  0.8 0.1 slice.12
  0.8 0.1 pad.4.clone
  0.9 0.7 multiply_convert_fusion.1
  1.7 0.1 pad_maximum_fusion
  1.7 4.9 %collective-permute-start = (bf16[64,128]{1,0:T(8,128)(2,1)S(1)}, bf16[64,128]{1,0:T(8,128)(2,1)S(1)}, u32[]{:S(2)}, u32[]{:S(2)}) collective-permute-start(bf16[64,128]{1,0:T(8,128)(2,1)S(1)} %pad_maximum_fusion), channel_id=1, source_target_pairs={{0,16},{16,32},{32,48},{48,64},{64,80},{80,96},{96,112},{112,128},... | collective-permute-start | bytes 49160 | tf_op jit(solution)/shard_map/ppermute | solution.py:340
  6.7 0.9 multiply_convert_fusion.gated
  7.6 0.7 pad_maximum_fusion.1.consts
  8.3 2.2 %collective-permute-done.halo = bf16[64,128]{1,0:T(8,128)(2,1)S(1)} collective-permute-done((bf16[64,128]{1,0:T(8,128)(2,1)S(1)}, bf16[64,128]{1,0:T(8,128)(2,1)S(1)}, u32[]{:S(2)}, u32[]{:S(2)}) %collective-permute-start) | collective-permute-done | bytes 16416 | tf_op jit(solution)/shard_map/ppermute | solution.py:340
  10.5 0.1 broadcast_in_dim.29.docs
  10.6 1.9 shard_map.127
  12.5 4.6 %all-to-all-start = ((bf16[16,272,128]{2,1,0:T(8,128)(2,1)}), bf16[16,272,128]{2,1,0:T(8,128)(2,1)S(1)}, u32[]{:S(2)}, u32[]{:S(2)}) async-start(bf16[16,272,128]{2,1,0:T(8,128)(2,1)} %shard_map.127), calls=%async_computation | async-start | bytes 2228224 | tf_op jit(solution)/shard_map/all_to_all | solution.py:274
  17.1 0.0 copy-done.13
  17.1 0.0 copy-done.14
  17.1 0.3 shard_map.128
  17.5 0.0 copy-start.10
  17.5 0.7 copy-done.10
  18.2 18.4 %all-to-all-done.parts = bf16[16,272,128]{2,1,0:T(8,128)(2,1)S(1)} async-done(((bf16[16,272,128]{2,1,0:T(8,128)(2,1)}), bf16[16,272,128]{2,1,0:T(8,128)(2,1)S(1)}, u32[]{:S(2)}, u32[]{:S(2)}) %all-to-all-start) | async-done | bytes 1114144 | tf_op jit(solution)/shard_map/all_to_all | solution.py:274
  36.6 0.0 copy-done.12
  36.6 2.0 shard_map.129
  38.6 36.2 %all_to_all.35 = bf16[32,32,128]{2,1,0:T(8,128)(2,1)S(1)} all-to-all(bf16[32,32,128]{2,1,0:T(8,128)(2,1)S(1)} %get-tuple-element.12), channel_id=1, replica_groups=mesh['sp'=32,'tp_0'=4,'tp_1'=4] {'sp'}, dimensions={0} | all-to-all | bytes 524288 | tf_op jit(solution)/shard_map/all_to_all | solution.py:274
  74.8 0.1 broadcast_in_dim.33
  74.9 9.3 %all_to_all.36 = bf16[4,512,128]{2,1,0:T(8,128)(2,1)S(1)} all-to-all(bf16[4,512,128]{2,1,0:T(8,128)(2,1)S(1)} %bitcast.26), channel_id=1, replica_groups={{0,1,2,3},{4,5,6,7},{8,9,10,11},{12,13,14,15},{16,20,24,28},{17,21,25,2..., dimensions={0} | all-to-all | bytes 1048576 | tf_op jit(solution)/shard_map/all_to_all | solution.py:287
  84.2 1.7 broadcast_in_dim.34
  86.0 3.7 %all-to-all-start.3 = ((bf16[4,4,512,128]{3,2,1,0:T(8,128)(2,1)}), bf16[4,4,512,128]{3,2,1,0:T(8,128)(2,1)S(1)}, u32[]{:S(2)}, u32[]{:S(2)}) async-start(bf16[4,4,512,128]{3,2,1,0:T(8,128)(2,1)} %broadcast_in_dim.34), calls=%async_computation.3 | async-start | bytes 4194304 | tf_op jit(solution)/shard_map/all_to_all | solution.py:287
  89.7 2.5 %collective-permute-start.1 = (bf16[2048,256]{1,0:T(8,128)(2,1)S(1)}, bf16[2048,256]{1,0:T(8,128)(2,1)S(1)}, u32[]{:S(2)}, u32[]{:S(2)}) collective-permute-start(bf16[2048,256]{1,0:T(8,128)(2,1)S(1)} %bitcast.16), channel_id=1, source_target_pairs={{0,1},{1,0},{2,3},{3,2},{4,5},{5,4},{6,7},{7,6},{8,9},{9,8},{10,11... | collective-permute-start | bytes 3145736 | tf_op jit(solution)/shard_map/ppermute | solution.py:303
  92.2 2.8 %collective-permute-start.2 = (bf16[2048,256]{1,0:T(8,128)(2,1)}, bf16[2048,256]{1,0:T(8,128)(2,1)S(1)}, u32[]{:S(2)}, u32[]{:S(2)}) collective-permute-start(bf16[2048,256]{1,0:T(8,128)(2,1)} %bitcast.18), channel_id=1, source_target_pairs={{0,1},{1,0},{2,3},{3,2},{4,5},{5,4},{6,7},{7,6},{8,9},{9,8},{10,11... | collective-permute-start | bytes 3145736 | tf_op jit(solution)/shard_map/ppermute | solution.py:303
  95.0 2.5 %collective-permute-start.3 = (bf16[256,2048]{1,0:T(8,128)(2,1)}, bf16[256,2048]{1,0:T(8,128)(2,1)S(1)}, u32[]{:S(2)}, u32[]{:S(2)}) collective-permute-start(bf16[256,2048]{1,0:T(8,128)(2,1)} %bitcast.20), channel_id=1, source_target_pairs={{0,1},{1,0},{2,3},{3,2},{4,5},{5,4},{6,7},{7,6},{8,9},{9,8},{10,11... | collective-permute-start | bytes 3145736 | tf_op jit(solution)/shard_map/ppermute | solution.py:303
  97.5 18.8 %collective-permute-done.1.gate_bh = bf16[2048,256]{1,0:T(8,128)(2,1)S(1)} collective-permute-done((bf16[2048,256]{1,0:T(8,128)(2,1)S(1)}, bf16[2048,256]{1,0:T(8,128)(2,1)S(1)}, u32[]{:S(2)}, u32[]{:S(2)}) %collective-permute-start.1) | collective-permute-done | bytes 1048608 | tf_op jit(solution)/shard_map/ppermute | solution.py:303
  116.3 1.0 copy-done.3
  117.2 10.8 %collective-permute-done.2.up_bh = bf16[2048,256]{1,0:T(8,128)(2,1)S(1)} collective-permute-done((bf16[2048,256]{1,0:T(8,128)(2,1)}, bf16[2048,256]{1,0:T(8,128)(2,1)S(1)}, u32[]{:S(2)}, u32[]{:S(2)}) %collective-permute-start.2) | collective-permute-done | bytes 1048608 | tf_op jit(solution)/shard_map/ppermute | solution.py:303
  128.0 1.0 copy-done.5
  129.0 9.9 %collective-permute-done.3.down_bh = bf16[256,2048]{1,0:T(8,128)(2,1)S(1)} collective-permute-done((bf16[256,2048]{1,0:T(8,128)(2,1)}, bf16[256,2048]{1,0:T(8,128)(2,1)S(1)}, u32[]{:S(2)}, u32[]{:S(2)}) %collective-permute-start.3) | collective-permute-done | bytes 1048608 | tf_op jit(solution)/shard_map/ppermute | solution.py:303
  139.0 1.0 copy-done.7
  139.9 0.0 all-to-all-done.3
  140.0 1.2 copy-done.1
  141.2 1.2 copy-done.2
  142.4 1.2 copy-done.4
  143.6 1.2 copy-done.6
  144.9 1.2 copy-done.8
  146.1 4.9 %shard_map.130 = bf16[16,512,128]{2,1,0:T(8,128)(2,1)S(1)} custom-call(bf16[16,512,128]{2,1,0:T(8,128)(2,1)S(1)} %bitcast.14, f32[16,128]{1,0:T(8,128)S(1)} %get-tuple-element.13.gains, bf16[2048,256]{1,0:T(8,128)(2,1)S(1)} %bitcast.17, bf16[2048,256]{1,0:T(8,128)(2,1)S(1)} %bitcast.19, bf16[256,2048]{1,0:T(8,128)(2,1)S(1)} %bitcast.21, ...), custom_call_target="tpu_custom_call" | custom-call | tf_op jit(solution)/shard_map/pallas_call | solution.py:383
  151.0 17.8 %all_to_all.37 = bf16[4,4,512,128]{3,2,1,0:T(8,128)(2,1)S(1)} all-to-all(bf16[4,4,512,128]{3,2,1,0:T(8,128)(2,1)S(1)} %bitcast.15), channel_id=1, replica_groups={{0,4,8,12},{1,5,9,13},{2,6,10,14},{3,7,11,15},{16,17,18,19},{20,21,22,2..., dimensions={0} | all-to-all | bytes 4194304 | tf_op jit(solution)/shard_map/all_to_all | solution.py:287
  168.8 0.6 reduce_sum.24
  169.4 10.1 %all_to_all.38 = bf16[4,512,128]{2,1,0:T(8,128)(2,1)S(1)} all-to-all(bf16[4,512,128]{2,1,0:T(8,128)(2,1)S(1)} %reduce_sum.24), channel_id=1, replica_groups={{0,1,2,3},{4,5,6,7},{8,9,10,11},{12,13,14,15},{16,20,24,28},{17,21,25,2..., dimensions={0} | all-to-all | bytes 1048576 | tf_op jit(solution)/shard_map/all_to_all | solution.py:287
  179.5 0.2 reduce_sum.25
  179.7 26.1 %all_to_all.39 = bf16[32,32,128]{2,1,0:T(8,128)(2,1)S(1)} all-to-all(bf16[32,32,128]{2,1,0:T(8,128)(2,1)S(1)} %bitcast.28), channel_id=1, replica_groups=mesh['sp'=32,'tp_0'=4,'tp_1'=4] {'sp'}, dimensions={0} | all-to-all | bytes 524288 | tf_op jit(solution)/shard_map/all_to_all | solution.py:274
  205.8 1.1 shard_map.131
  (16 shorter events, 0.0 us)
Async XLA Ops:
  0.0 17.1 %copy-start.13 = (s32[256,2]{0,1:T(2,128)S(1)}, s32[256,2]{0,1:T(2,128)}, u32[]{:S(2)}) copy-start(s32[256,2]{0,1:T(2,128)} %param.21) | copy-start | bytes 6148
  0.0 17.1 %copy-start.14 = (f32[256,2]{0,1:T(2,128)S(1)}, f32[256,2]{0,1:T(2,128)}, u32[]{:S(2)}) copy-start(f32[256,2]{0,1:T(2,128)} %param.22) | copy-start | bytes 6148
  0.0 36.6 %copy-start.12 = (bf16[256,128]{1,0:T(8,128)(2,1)S(1)}, bf16[256,128]{1,0:T(8,128)(2,1)}, u32[]{:S(2)}) copy-start(bf16[256,128]{1,0:T(8,128)(2,1)} %residual.1) | copy-start | bytes 196612
  0.0 36.6 %copy-start.9 = (bf16[2048,128]{1,0:T(8,128)(2,1)S(1)}, bf16[2048,128]{1,0:T(8,128)(2,1)}, u32[]{:S(2)}) copy-start(bf16[2048,128]{1,0:T(8,128)(2,1)} %out_weight.1) | copy-start | bytes 1572868
  1.7 8.8 %collective-permute-start = (bf16[64,128]{1,0:T(8,128)(2,1)S(1)}, bf16[64,128]{1,0:T(8,128)(2,1)S(1)}, u32[]{:S(2)}, u32[]{:S(2)}) collective-permute-start(bf16[64,128]{1,0:T(8,128)(2,1)S(1)} %pad_maximum_fusion), channel_id=1, source_target_pairs={{0,16},{16,32},{32,48},{48,64},{64,80},{80,96},{96,112},{112,128},... | collective-permute-start | bytes 49160 | tf_op jit(solution)/shard_map/ppermute | solution.py:340
  12.5 24.1 %all-to-all-start = ((bf16[16,272,128]{2,1,0:T(8,128)(2,1)}), bf16[16,272,128]{2,1,0:T(8,128)(2,1)S(1)}, u32[]{:S(2)}, u32[]{:S(2)}) async-start(bf16[16,272,128]{2,1,0:T(8,128)(2,1)} %shard_map.127), calls=%async_computation | async-start | bytes 2228224 | tf_op jit(solution)/shard_map/all_to_all | solution.py:274
  17.5 0.7 copy-start.10
  86.0 3.8 %copy-start = (bf16[1,2048,256]{2,1,0:T(8,128)(2,1)S(1)}, bf16[1,2048,256]{2,1,0:T(8,128)(2,1)}, u32[]{:S(2)}) copy-start(bf16[1,2048,256]{2,1,0:T(8,128)(2,1)} %param.23) | copy-start | bytes 3145732
  86.0 54.0 %all-to-all-start.3 = ((bf16[4,4,512,128]{3,2,1,0:T(8,128)(2,1)}), bf16[4,4,512,128]{3,2,1,0:T(8,128)(2,1)S(1)}, u32[]{:S(2)}, u32[]{:S(2)}) async-start(bf16[4,4,512,128]{3,2,1,0:T(8,128)(2,1)} %broadcast_in_dim.34), calls=%async_computation.3 | async-start | bytes 4194304 | tf_op jit(solution)/shard_map/all_to_all | solution.py:287
  89.7 26.5 %collective-permute-start.1 = (bf16[2048,256]{1,0:T(8,128)(2,1)S(1)}, bf16[2048,256]{1,0:T(8,128)(2,1)S(1)}, u32[]{:S(2)}, u32[]{:S(2)}) collective-permute-start(bf16[2048,256]{1,0:T(8,128)(2,1)S(1)} %bitcast.16), channel_id=1, source_target_pairs={{0,1},{1,0},{2,3},{3,2},{4,5},{5,4},{6,7},{7,6},{8,9},{9,8},{10,11... | collective-permute-start | bytes 3145736 | tf_op jit(solution)/shard_map/ppermute | solution.py:303
  92.2 35.8 %collective-permute-start.2 = (bf16[2048,256]{1,0:T(8,128)(2,1)}, bf16[2048,256]{1,0:T(8,128)(2,1)S(1)}, u32[]{:S(2)}, u32[]{:S(2)}) collective-permute-start(bf16[2048,256]{1,0:T(8,128)(2,1)} %bitcast.18), channel_id=1, source_target_pairs={{0,1},{1,0},{2,3},{3,2},{4,5},{5,4},{6,7},{7,6},{8,9},{9,8},{10,11... | collective-permute-start | bytes 3145736 | tf_op jit(solution)/shard_map/ppermute | solution.py:303
  95.0 43.9 %collective-permute-start.3 = (bf16[256,2048]{1,0:T(8,128)(2,1)}, bf16[256,2048]{1,0:T(8,128)(2,1)S(1)}, u32[]{:S(2)}, u32[]{:S(2)}) collective-permute-start(bf16[256,2048]{1,0:T(8,128)(2,1)} %bitcast.20), channel_id=1, source_target_pairs={{0,1},{1,0},{2,3},{3,2},{4,5},{5,4},{6,7},{7,6},{8,9},{9,8},{10,11... | collective-permute-start | bytes 3145736 | tf_op jit(solution)/shard_map/ppermute | solution.py:303
  116.3 1.0 copy-start.3
  128.0 1.0 copy-start.5
  139.0 1.0 copy-start.7
  140.0 1.2 copy-start.1
  141.2 1.2 copy-start.2
  142.4 1.2 copy-start.4
  143.6 1.2 copy-start.6
  144.9 1.2 copy-start.8
  168.8 37.0 %copy-start.11 = (f32[2,256,128]{2,1,0:T(8,128)S(1)}, f32[2,256,128]{2,1,0:T(8,128)}, u32[]{:S(2)}) copy-start(f32[2,256,128]{2,1,0:T(8,128)} %copy-done.10) | copy-start | bytes 786436
